TPU v7x, 32 devices: a whole 2x2x4 slice. The times are simulated.
32 devices in a mesh: sp: 8 (over z, y), tp: 4 (over x, core).
Axes of the slice: x: 2, y: 2, z: 4, core: 2. Of those that a mesh axis runs over, the one named last changes fastest.
Arguments:
- expert_input: bfloat16 [3072, 2048], P('sp'), may hold values from -6 to 6
- cotangent: bfloat16 [3072, 2048], P('sp'), may hold values from -6 to 6
- routes: int32 [3072, 2], P('sp'), may hold values from 0 to 7, all different within a row; in each aligned block of 384 rows (0 to 383, 384 to 767, ...) at most 144 rows name the same one
- route_weight: float32 [3072, 2], P('sp'), may hold values from 0.2 to 2.5
- expert_gate: bfloat16 [8, 2048, 1024], P('sp', None, 'tp'), may hold values from -0.125 to 0.125
- expert_up: bfloat16 [8, 2048, 1024], P('sp', None, 'tp'), may hold values from -0.125 to 0.125
- expert_down: bfloat16 [8, 1024, 2048], P('sp', 'tp'), may hold values from -0.1875 to 0.1875
- conv_out: bfloat16 [3072, 1024], P('sp', 'tp'), may hold values from -14 to 14
- conv_value: bfloat16 [3072, 1024], P('sp', 'tp'), may hold values from -6 to 6
- conv_gate: bfloat16 [3072, 1024], P('sp', 'tp'), may hold values from -6 to 6
- conv_taps: float32 [31, 1024], P(None, 'tp'), may hold values from -1 to 1
- norm_gain: float32 [1024], P('tp'), may hold values from 0.1 to 1.9
- norm_bias: float32 [1024], P('tp'), may hold values from -3 to 3
- out_weight: bfloat16 [1024, 2048], P('tp'), may hold values from -0.1875 to 0.1875
Outputs:
- gate_grad: float32 [8, 2048, 1024], P('sp', None, 'tp')
- up_grad: float32 [8, 2048, 1024], P('sp', None, 'tp')
- down_grad: float32 [8, 1024, 2048], P('sp', 'tp')
- resid_grad: bfloat16 [3072, 2048], P('sp')
- out_weight_grad: float32 [1024, 2048], P('tp', 'sp')
- value_grad: bfloat16 [3072, 1024], P('sp', 'tp')
- gate_in_grad: bfloat16 [3072, 1024], P('sp', 'tp')
Inputs may be any that keep to these rules, and one draw needn't show every extreme that they name: `routes`: each token names 2 different experts. In each aligned block of 384 tokens no expert is named by more than 144 tokens, and in every draw some block has an expert named by exactly 144 tokens.
All inputs are finite; a program needn't handle non-finite values.
Results may differ from a plain program's by a relative error of at most 0.018.
Values may be sent and summed in bfloat16 or wider, within the bound.
A program may use at most 128 MiB of HBM per device.

v0:
```python
import jax
import jax.numpy as jnp
from jax import lax
from jax.sharding import PartitionSpec as P

norm_eps = 1e-06


def passed_along(value, axis, steps):
    count = lax.axis_size(axis)
    leading, last = (max(0, -steps), min(count, count - steps))
    return lax.ppermute(value, axis, [(source, source + steps) for source in range(leading, last)])


def on_device(
    expert_input,
    cotangent,
    routes,
    route_weight,
    expert_gate,
    expert_up,
    expert_down,
    conv_out,
    conv_value,
    conv_gate,
    conv_taps,
    norm_gain,
    norm_bias,
    out_weight,
):
    sp_count = lax.axis_size("sp")
    tp_count = lax.axis_size("tp")
    tok_rows, model_width = expert_input.shape
    share_cols = model_width // tp_count
    top_count = routes.shape[1]
    local_exp = expert_gate.shape[0]
    experts = local_exp * sp_count
    capacity = 3 * top_count * tok_rows // (2 * experts)
    assigns = tok_rows * top_count
    flat_routes = routes.reshape(assigns)
    onehot = (flat_routes[:, None] == jnp.arange(experts, dtype=jnp.int32)[None, :]).astype(
        jnp.int32
    )
    slot_rank = jnp.sum((jnp.cumsum(onehot, axis=0) - onehot) * onehot, axis=1)
    target = flat_routes * capacity + slot_rank
    slot_ids = (
        jnp.full((experts * capacity,), assigns, jnp.int32)
        .at[target]
        .set(jnp.arange(assigns, dtype=jnp.int32))
    )
    token_of = slot_ids // top_count
    padded_in = jnp.concatenate([expert_input, jnp.zeros((1, model_width), jnp.bfloat16)], axis=0)
    padded_cot = jnp.concatenate([cotangent, jnp.zeros((1, model_width), jnp.bfloat16)], axis=0)
    padded_weight = jnp.concatenate(
        [route_weight.reshape(assigns), jnp.zeros((1,), jnp.float32)], axis=0
    )
    send_rows = padded_in[token_of].reshape(experts, capacity, model_width)
    send_cot = (padded_cot[token_of].astype(jnp.float32) * padded_weight[slot_ids][:, None]).astype(
        jnp.bfloat16
    )
    send_cot = send_cot.reshape(experts, capacity, model_width)
    got_rows, got_cot = (
        lax.all_to_all(send_rows, "sp", split_axis=0, concat_axis=0, tiled=True),
        lax.all_to_all(send_cot, "sp", split_axis=0, concat_axis=0, tiled=True),
    )

    def by_expert(arrived):
        return (
            arrived.reshape(sp_count, local_exp, capacity, model_width)
            .transpose(1, 0, 2, 3)
            .reshape(local_exp, sp_count * capacity, model_width)
        )

    slot_rows = by_expert(got_rows)
    slot_cots = by_expert(got_cot)
    pre_gate = jnp.einsum(
        "lrd,ldf->lrf", slot_rows, expert_gate, preferred_element_type=jnp.float32
    )
    pre_up = jnp.einsum("lrd,ldf->lrf", slot_rows, expert_up, preferred_element_type=jnp.float32)
    gate_sig = jax.nn.sigmoid(pre_gate)
    gate_act = pre_gate * gate_sig
    hidden = (gate_act * pre_up).astype(jnp.bfloat16)
    hidden_grad = jnp.einsum(
        "lrd,lfd->lrf", slot_cots, expert_down, preferred_element_type=jnp.float32
    )
    down_grad = jnp.einsum("lrf,lrd->lfd", hidden, slot_cots, preferred_element_type=jnp.float32)
    gate_pre = (hidden_grad * pre_up * gate_sig * (1.0 + pre_gate * (1.0 - gate_sig))).astype(
        jnp.bfloat16
    )
    up_pre = (hidden_grad * gate_act).astype(jnp.bfloat16)
    gate_grad = jnp.einsum("lrd,lrf->ldf", slot_rows, gate_pre, preferred_element_type=jnp.float32)
    up_grad = jnp.einsum("lrd,lrf->ldf", slot_rows, up_pre, preferred_element_type=jnp.float32)
    partial_rows = jnp.einsum(
        "lrf,ldf->lrd", gate_pre, expert_gate, preferred_element_type=jnp.float32
    )
    partial_rows = partial_rows + jnp.einsum(
        "lrf,ldf->lrd", up_pre, expert_up, preferred_element_type=jnp.float32
    )
    partial_src = (
        partial_rows.reshape(local_exp, sp_count, capacity, model_width)
        .transpose(1, 0, 2, 3)
        .reshape(experts, capacity, model_width)
    )
    partial_low = partial_src.astype(jnp.bfloat16)
    row_share = lax.psum_scatter(partial_low, "tp", scatter_dimension=2, tiled=True).astype(
        jnp.float32
    )
    slot_back = lax.all_to_all(
        row_share.astype(jnp.bfloat16), "sp", split_axis=0, concat_axis=0, tiled=True
    )
    picked = slot_back.reshape(experts * capacity, share_cols)[target].astype(jnp.float32)
    combined = jnp.sum(picked.reshape(tok_rows, top_count, share_cols), axis=1)
    own_cot = lax.dynamic_slice_in_dim(cotangent, lax.axis_index("tp") * share_cols, share_cols, 1)
    resid_part = (own_cot.astype(jnp.float32) + combined).astype(jnp.bfloat16)
    resid_grad = lax.all_gather(resid_part, "tp", axis=1, tiled=True)
    mix_grad = lax.dot_general(
        resid_grad, out_weight, (((1,), (1,)), ((), ())), preferred_element_type=jnp.float32
    )
    channels = conv_out.shape[1] * tp_count
    conv_vals = conv_out.astype(jnp.float32)
    row_sum, row_square = lax.psum(
        (jnp.sum(conv_vals, axis=1), jnp.sum(conv_vals * conv_vals, axis=1)), "tp"
    )
    row_mean = (row_sum / channels)[:, None]
    row_var = (row_square / channels)[:, None] - row_mean * row_mean
    row_rstd = lax.rsqrt(row_var + norm_eps)
    normed = (conv_vals - row_mean) * row_rstd
    norm_pre = normed * norm_gain[None, :] + norm_bias[None, :]
    norm_sig = jax.nn.sigmoid(norm_pre)
    conv_act = (norm_pre * norm_sig).astype(jnp.bfloat16)
    norm_grad = mix_grad * norm_sig * (1.0 + norm_pre * (1.0 - norm_sig)) * norm_gain[None, :]
    grad_sum, grad_dot = lax.psum(
        (jnp.sum(norm_grad, axis=1), jnp.sum(norm_grad * normed, axis=1)), "tp"
    )
    conv_grad = row_rstd * (
        norm_grad - (grad_sum / channels)[:, None] - normed * (grad_dot / channels)[:, None]
    )
    taps_count = conv_taps.shape[0]
    next_rows = passed_along(conv_grad[: taps_count - 1], "sp", -1)
    extended = jnp.concatenate([conv_grad, next_rows], axis=0)
    glu_grad = jnp.zeros_like(conv_grad)
    for lag_index in range(taps_count):
        begin = taps_count - 1 - lag_index
        glu_grad = glu_grad + conv_taps[lag_index][None, :] * extended[begin : begin + tok_rows]
    gate_sig_in = jax.nn.sigmoid(conv_gate.astype(jnp.float32))
    value_grad = (glu_grad * gate_sig_in).astype(jnp.bfloat16)
    gate_in_grad = (
        glu_grad * conv_value.astype(jnp.float32) * gate_sig_in * (1.0 - gate_sig_in)
    ).astype(jnp.bfloat16)
    projected = lax.psum_scatter(
        lax.dot_general(
            resid_grad, conv_act, (((0,), (0,)), ((), ())), preferred_element_type=jnp.float32
        ).astype(jnp.bfloat16),
        "sp",
        scatter_dimension=0,
        tiled=True,
    ).astype(jnp.float32)
    out_weight_grad = projected.T
    return (gate_grad, up_grad, down_grad, resid_grad, out_weight_grad, value_grad, gate_in_grad)


def solution(mesh):
    return jax.shard_map(
        on_device,
        mesh=mesh,
        in_specs=(
            P("sp", None),
            P("sp", None),
            P("sp", None),
            P("sp", None),
            P("sp", None, "tp"),
            P("sp", None, "tp"),
            P("sp", "tp", None),
            P("sp", "tp"),
            P("sp", "tp"),
            P("sp", "tp"),
            P(None, "tp"),
            P("tp"),
            P("tp"),
            P("tp", None),
        ),
        out_specs=(
            P("sp", None, "tp"),
            P("sp", None, "tp"),
            P("sp", "tp", None),
            P("sp", None),
            P("tp", "sp"),
            P("sp", "tp"),
            P("sp", "tp"),
        ),
        check_vma=False,
    )
```

profile of v0, /device:TPU:0, one launch (start us, length us, event | category | flops | bytes accessed | tf_op | source)
XLA Modules:
  0.0 437.1 jit_solution(16315838665781206947)
XLA Ops:
  7.2 0.0 copy-start
  7.2 0.8 broadcast_multiply_fusion
  8.0 0.8 copy.25
  8.8 0.1 eq.29
  8.9 0.1 eq.25
  9.1 0.1 copy.24
  9.2 0.2 mul.443
  9.4 1.7 reduce-window.6
  11.1 0.1 slice.264
  11.2 0.1 copy.27
  11.3 0.2 reduce-window.9
  11.5 0.1 copy.28
  11.6 0.1 fusion.128
  11.7 3.4 scatter_custom_fusion
  15.1 1.5 concatenate.12
  16.6 6.0 %gather_fusion = bf16[1152,2048]{1,0:T(8,128)(2,1)} fusion(bf16[385,2048]{1,0:T(8,128)(2,1)S(1)} %concatenate.12, s32[2048]{0:T(1024)S(1)} %get-tuple-element.70), kind=kCustom, calls=%fused_computation | custom fusion | bytes 9441792 | tf_op jit(solution)/shard_map/gather | solution.py:57
  22.7 7.3 %all-to-all-start = ((bf16[8,144,2048]{2,1,0:T(8,128)(2,1)}), bf16[8,144,2048]{2,1,0:T(8,128)(2,1)}, u32[]{:S(2)}, u32[]{:S(2)}) async-start(bf16[8,144,2048]{2,1,0:T(8,128)(2,1)} %bitcast.85), calls=%async_computation | async-start | bytes 9437184 | tf_op jit(solution)/shard_map/all_to_all | solution.py:63
  30.0 1.5 concatenate.13
  31.5 5.9 %gather_fusion.1 = bf16[1152,2048]{1,0:T(8,128)(2,1)} fusion(bf16[385,2048]{1,0:T(8,128)(2,1)S(1)} %concatenate.13, s32[2048]{0:T(1024)S(1)} %get-tuple-element.70), kind=kCustom, calls=%fused_computation.1 | custom fusion | bytes 9441792 | tf_op jit(solution)/shard_map/gather | solution.py:58
  37.4 0.1 copy.29
  37.6 0.1 reshape.160
  37.7 4.6 %gather_fusion.2 = f32[1152]{0:T(1024)S(1)} fusion(f32[769]{0:T(1024)S(1)} %pad_maximum_fusion.1, s32[2048]{0:T(1024)S(1)} %get-tuple-element.69), kind=kCustom, calls=%fused_computation.2 | custom fusion | bytes 13824 | tf_op jit(solution)/shard_map/gather | solution.py:58
  42.3 0.1 mul.445
  42.4 5.4 %fusion = bf16[8,144,2048]{2,1,0:T(8,128)(2,1)} fusion(bf16[8,144,2048]{2,1,0:T(8,128)(2,1)} %bitcast.87, f32[8,144]{1,0:T(8,128)S(1)} %mul.445), kind=kLoop, calls=%fused_computation.7 | loop fusion | flops 7077888 | bytes 9441792 | tf_op jit(solution)/shard_map/convert_element_type | solution.py:58
  47.8 86.7 %all-to-all-done = bf16[8,144,2048]{2,1,0:T(8,128)(2,1)} async-done(((bf16[8,144,2048]{2,1,0:T(8,128)(2,1)}), bf16[8,144,2048]{2,1,0:T(8,128)(2,1)}, u32[]{:S(2)}, u32[]{:S(2)}) %all-to-all-start) | async-done | bytes 4718624 | tf_op jit(solution)/shard_map/all_to_all | solution.py:63
  134.5 4.6 %all-to-all-start.1 = ((bf16[8,144,2048]{2,1,0:T(8,128)(2,1)}), bf16[8,144,2048]{2,1,0:T(8,128)(2,1)}, u32[]{:S(2)}, u32[]{:S(2)}) async-start(bf16[8,144,2048]{2,1,0:T(8,128)(2,1)} %fusion), calls=%async_computation.1 | async-start | bytes 9437184 | tf_op jit(solution)/shard_map/all_to_all | solution.py:64
  139.1 0.2 reduce-scatter.3.cloned.1.call-start
  139.3 0.0 copy-start.4
  139.3 4.8 %fusion.7 = f32[1152,256]{1,0:T(8,128)} fusion(bf16[1152,2048]{1,0:T(8,128)(2,1)} %bitcast.4, bf16[1,2048,256]{2,1,0:T(8,128)(2,1)S(1)} %copy-done), kind=kOutput, calls=%fused_computation.52 | convolution fusion | flops 1207959552 | bytes 6946816 | tf_op jit(solution)/shard_map/lrd,ldf->lrf/dot_general | solution.py:76
  144.2 4.7 %fusion.10 = f32[1152,256]{1,0:T(8,128)} fusion(bf16[1152,2048]{1,0:T(8,128)(2,1)} %bitcast.4, bf16[1,2048,256]{2,1,0:T(8,128)(2,1)S(1)} %copy-done.4), kind=kOutput, calls=%fused_computation.55 | convolution fusion | flops 1207959552 | bytes 6946816 | tf_op jit(solution)/shard_map/lrd,ldf->lrf/dot_general | solution.py:79
  148.9 93.9 %all-to-all-done.1 = bf16[8,144,2048]{2,1,0:T(8,128)(2,1)} async-done(((bf16[8,144,2048]{2,1,0:T(8,128)(2,1)}), bf16[8,144,2048]{2,1,0:T(8,128)(2,1)}, u32[]{:S(2)}, u32[]{:S(2)}) %all-to-all-start.1) | async-done | bytes 4718624 | tf_op jit(solution)/shard_map/all_to_all | solution.py:64
  242.8 5.0 %multiply_convert_fusion.1 = (bf16[1152,256]{1,0:T(8,128)(2,1)S(1)}, bf16[1152,256]{1,0:T(8,128)(2,1)S(1)}) fusion(f32[1152,256]{1,0:T(8,128)} %fusion.7, f32[1152,256]{1,0:T(8,128)} %fusion.10, bf16[1152,2048]{1,0:T(8,128)(2,1)} %bitcast.6, bf16[1,256,2048]{2,1,0:T(8,128)(2,1)} %param.20), kind=kOutput, calls=%fused_computation.46 | convolution fusion | flops 1211793408 | bytes 9306112 | tf_op jit(solution)/shard_map/lrd,lfd->lrf/dot_general | solution.py:83
  247.9 1.4 fusion.5
  249.3 3.7 fusion.1
  253.0 0.0 reduce-scatter.3.cloned.1.call-update
  253.0 47.0 %reduce-scatter.3.cloned.1.call-done = bf16[8,144,512]{2,1,0:T(8,128)(2,1)} async-done(((bf16[8,144,2048]{2,1,0:T(8,128)(2,1)}), bf16[8,144,512]{2,1,0:T(8,128)(2,1)}) %reduce-scatter.3.cloned.1.call-update) | async-done | bytes 1179664 | tf_op jit(solution)/shard_map/reduce_scatter | solution.py:105
  300.1 5.5 %all-to-all-start.2 = ((bf16[8,144,512]{2,1,0:T(8,128)(2,1)}), bf16[8,144,512]{2,1,0:T(8,128)(2,1)S(1)}, u32[]{:S(2)}, u32[]{:S(2)}) async-start(bf16[8,144,512]{2,1,0:T(8,128)(2,1)} %reduce-scatter.3.cloned.1.call-done), calls=%async_computation.3 | async-start | bytes 2359296 | tf_op jit(solution)/shard_map/all_to_all | solution.py:108
  305.6 0.0 all-gather.2.cloned.1.call-start
  305.7 28.3 %all-to-all-done.2 = bf16[8,144,512]{2,1,0:T(8,128)(2,1)S(1)} async-done(((bf16[8,144,512]{2,1,0:T(8,128)(2,1)}), bf16[8,144,512]{2,1,0:T(8,128)(2,1)S(1)}, u32[]{:S(2)}, u32[]{:S(2)}) %all-to-all-start.2) | async-done | bytes 1179680 | tf_op jit(solution)/shard_map/all_to_all | solution.py:108
  334.0 2.7 gather_fusion.3
  336.7 1.0 reshape.167
  337.6 1.9 reduce_sum.58
  339.6 2.0 add_convert_fusion
  341.5 0.0 all-gather.2.cloned.1.call-update
  341.5 0.0 reduce-scatter.5.cloned.1.call-start
  341.6 0.2 convert_reduce_fusion
  341.8 6.2 %all-reduce.3 = (f32[384]{0:T(512)S(1)}, f32[384]{0:T(512)S(1)}) all-reduce(f32[384]{0:T(512)S(1)} %get-tuple-element.24, f32[384]{0:T(512)S(1)} %get-tuple-element.23), channel_id=1, replica_groups=mesh['sp'=8,'tp'=4] {'tp'}, use_global_device_ids=true, to_apply=%region_9.10 | all-reduce | flops 768 | bytes 6144 | tf_op jit(solution)/shard_map/psum | solution.py:121
  348.1 5.4 %convolution_bitcast_fusion.2 = f32[1,2048,256]{2,1,0:T(8,128)} fusion(bf16[1152,2048]{1,0:T(8,128)(2,1)} %bitcast.4, bf16[1152,256]{1,0:T(8,128)(2,1)S(1)} %copy-done.3), kind=kOutput, calls=%fused_computation.40 | convolution fusion | flops 1207959552 | bytes 7405568 | tf_op jit(solution)/shard_map/lrd,lrf->ldf/dot_general | solution.py:91
  353.5 5.4 %convolution_bitcast_fusion = f32[1,256,2048]{2,1,0:T(8,128)} fusion(bf16[1152,2048]{1,0:T(8,128)(2,1)} %bitcast.6, f32[1152,256]{1,0:T(8,128)S(1)} %copy-done.16, f32[1152,256]{1,0:T(8,128)S(1)} %copy-done.15), kind=kOutput, calls=%fused_computation.38 | convolution fusion | flops 1209729024 | bytes 9175040 | tf_op jit(solution)/shard_map/lrf,lrd->lfd/dot_general | solution.py:86
  358.8 0.6 all-gather.2.cloned.1.call-done
  359.5 3.4 convolution_convert_fusion
  362.9 0.0 reduce-scatter.5.cloned.1.call-update
  362.9 2.7 fusion.137
  365.6 6.4 %all-reduce.2 = (f32[384]{0:T(512)}, f32[384]{0:T(512)S(1)}) all-reduce(f32[384]{0:T(512)S(1)} %get-tuple-element.22, f32[384]{0:T(512)S(1)} %get-tuple-element.21), channel_id=1, replica_groups=mesh['sp'=8,'tp'=4] {'tp'}, use_global_device_ids=true, to_apply=%region_14.15 | all-reduce | flops 768 | bytes 6144 | tf_op jit(solution)/shard_map/psum | solution.py:132
  372.0 0.7 broadcast_multiply_fusion.1
  372.7 1.3 fusion.29
  374.0 1.4 collective-permute-start
  375.5 5.2 %convolution_bitcast_fusion.1 = f32[1,2048,256]{2,1,0:T(8,128)} fusion(bf16[1152,2048]{1,0:T(8,128)(2,1)} %bitcast.4, bf16[1152,256]{1,0:T(8,128)(2,1)S(1)} %copy-done.9), kind=kOutput, calls=%fused_computation.39 | convolution fusion | flops 1207959552 | bytes 7405568 | tf_op jit(solution)/shard_map/lrd,lrf->ldf/dot_general | solution.py:92
  380.7 2.7 multiply_convert_fusion.4
  383.5 0.8 multiply_convert_fusion.5
  384.2 43.5 %reduce-scatter.5.cloned.1.call-done = bf16[256,256]{1,0:T(8,128)(2,1)} async-done(((bf16[2048,256]{1,0:T(8,128)(2,1)}), bf16[256,256]{1,0:T(8,128)(2,1)}) %reduce-scatter.5.cloned.1.call-update) | async-done | bytes 131088 | tf_op jit(solution)/shard_map/reduce_scatter | solution.py:150
  427.7 0.9 convert_bitcast_fusion
  428.6 0.8 copy.30
  429.5 1.1 copy.32
  (45 shorter events, 0.2 us)
Async XLA Ops:
  7.2 132.2 %copy-start = (bf16[1,2048,256]{2,1,0:T(8,128)(2,1)S(1)}, bf16[1,2048,256]{2,1,0:T(8,128)(2,1)}, u32[]{:S(2)}) copy-start(bf16[1,2048,256]{2,1,0:T(8,128)(2,1)} %param.18) | copy-start | bytes 3145732
  22.7 111.8 %all-to-all-start = ((bf16[8,144,2048]{2,1,0:T(8,128)(2,1)}), bf16[8,144,2048]{2,1,0:T(8,128)(2,1)}, u32[]{:S(2)}, u32[]{:S(2)}) async-start(bf16[8,144,2048]{2,1,0:T(8,128)(2,1)} %bitcast.85), calls=%async_computation | async-start | bytes 9437184 | tf_op jit(solution)/shard_map/all_to_all | solution.py:63
  31.5 5.9 %copy-start.12 = (f32[384,2]{0,1:T(2,128)S(1)}, f32[384,2]{0,1:T(2,128)}, u32[]{:S(2)}) copy-start(f32[384,2]{0,1:T(2,128)} %param.17) | copy-start | bytes 9220
  134.5 108.3 %all-to-all-start.1 = ((bf16[8,144,2048]{2,1,0:T(8,128)(2,1)}), bf16[8,144,2048]{2,1,0:T(8,128)(2,1)}, u32[]{:S(2)}, u32[]{:S(2)}) async-start(bf16[8,144,2048]{2,1,0:T(8,128)(2,1)} %fusion), calls=%async_computation.1 | async-start | bytes 9437184 | tf_op jit(solution)/shard_map/all_to_all | solution.py:64
  139.1 161.0 %reduce-scatter.3.cloned.1.call-start = ((), (), s32[]{:S(2)}) async-start(), calls=%async_computation.5 | async-start | bytes 5898240 | tf_op jit(solution)/shard_map/reduce_scatter | solution.py:105
  139.3 4.8 %copy-start.4 = (bf16[1,2048,256]{2,1,0:T(8,128)(2,1)S(1)}, bf16[1,2048,256]{2,1,0:T(8,128)(2,1)}, u32[]{:S(2)}) copy-start(bf16[1,2048,256]{2,1,0:T(8,128)(2,1)} %param.19) | copy-start | bytes 3145732
  247.9 1.5 copy-start.2
  247.9 1.5 copy-start.8
  300.1 33.9 %all-to-all-start.2 = ((bf16[8,144,512]{2,1,0:T(8,128)(2,1)}), bf16[8,144,512]{2,1,0:T(8,128)(2,1)S(1)}, u32[]{:S(2)}, u32[]{:S(2)}) async-start(bf16[8,144,512]{2,1,0:T(8,128)(2,1)} %reduce-scatter.3.cloned.1.call-done), calls=%async_computation.3 | async-start | bytes 2359296 | tf_op jit(solution)/shard_map/all_to_all | solution.py:108
  305.6 53.9 %all-gather.2.cloned.1.call-start = ((), (), s32[]{:S(2)}) async-start(), calls=%async_computation.6 | async-start | bytes 1966080 | tf_op jit(solution)/shard_map/all_gather | solution.py:115
  339.5 2.1 copy-start.6
  339.5 8.5 %copy-start.11 = (f32[31,256]{1,0:T(8,128)S(1)}, f32[31,256]{1,0:T(8,128)}, u32[]{:S(2)}) copy-start(f32[31,256]{1,0:T(8,128)} %param.24) | copy-start | bytes 95236
  339.5 8.5 %copy-start.3 = (bf16[1152,256]{1,0:T(8,128)(2,1)S(1)}, bf16[1152,256]{1,0:T(8,128)(2,1)}, u32[]{:S(2)}) copy-start(bf16[1152,256]{1,0:T(8,128)(2,1)} %copy-done.2) | copy-start | bytes 1769476
  341.5 86.2 %reduce-scatter.5.cloned.1.call-start = ((), (), s32[]{:S(2)}) async-start(), calls=%async_computation.7 | async-start | bytes 1179648 | tf_op jit(solution)/shard_map/reduce_scatter | solution.py:150
  348.0 5.4 %copy-start.15 = (f32[1152,256]{1,0:T(8,128)S(1)}, f32[1152,256]{1,0:T(8,128)}, u32[]{:S(2)}) copy-start(f32[1152,256]{1,0:T(8,128)} %fusion.7) | copy-start | bytes 3538948
  348.1 5.4 %copy-start.16 = (f32[1152,256]{1,0:T(8,128)S(1)}, f32[1152,256]{1,0:T(8,128)}, u32[]{:S(2)}) copy-start(f32[1152,256]{1,0:T(8,128)} %fusion.10) | copy-start | bytes 3538948
  353.4 6.0 %copy-start.7 = (bf16[384,256]{1,0:T(8,128)(2,1)S(1)}, bf16[384,256]{1,0:T(8,128)(2,1)}, u32[]{:S(2)}) copy-start(bf16[384,256]{1,0:T(8,128)(2,1)} %param.21) | copy-start | bytes 589828
  353.4 6.0 %copy-start.13 = (f32[256]{0:T(256)S(1)}, f32[256]{0:T(256)}, u32[]{:S(2)}) copy-start(f32[256]{0:T(256)} %param.26) | copy-start | bytes 3076
  353.5 6.0 %copy-start.14 = (f32[256]{0:T(256)S(1)}, f32[256]{0:T(256)}, u32[]{:S(2)}) copy-start(f32[256]{0:T(256)} %param.25) | copy-start | bytes 3076
  359.5 3.4 copy-start.1
  362.9 12.5 %copy-start.9 = (bf16[1152,256]{1,0:T(8,128)(2,1)S(1)}, bf16[1152,256]{1,0:T(8,128)(2,1)}, u32[]{:S(2)}) copy-start(bf16[1152,256]{1,0:T(8,128)(2,1)} %copy-done.8) | copy-start | bytes 1769476
  374.0 6.7 %copy-start.5 = (bf16[384,256]{1,0:T(8,128)(2,1)S(1)}, bf16[384,256]{1,0:T(8,128)(2,1)}, u32[]{:S(2)}) copy-start(bf16[384,256]{1,0:T(8,128)(2,1)} %param.23) | copy-start | bytes 589828
  374.0 6.7 %copy-start.10 = (bf16[384,256]{1,0:T(8,128)(2,1)S(1)}, bf16[384,256]{1,0:T(8,128)(2,1)}, u32[]{:S(2)}) copy-start(bf16[384,256]{1,0:T(8,128)(2,1)} %param.22) | copy-start | bytes 589828
  374.0 6.7 %collective-permute-start = (f32[30,256]{1,0:T(8,128)S(1)}, f32[30,256]{1,0:T(8,128)S(1)}, u32[]{:S(2)}, u32[]{:S(2)}) collective-permute-start(f32[30,256]{1,0:T(8,128)S(1)} %slice.265), channel_id=1, source_target_pairs={{4,0},{8,4},{12,8},{16,12},{20,16},{24,20},{28,24},{5,1},{9,5},{13... | collective-permute-start | bytes 92168 | tf_op jit(solution)/shard_map/ppermute | solution.py:12
Sparse Core Ops, SparseCore 0:
  253.2 46.8 reduce-scatter.2
  341.7 17.7 all-gather.1
  363.4 64.2 reduce-scatter.4
where the time goes:
time: 438 us; the launch traced here: 437 us
  waiting for transfers between devices  300 us (68%)
  matrix products  41.8 us (10%)
  local copies, waits for them, and re-layouts  30.7 us (7%)
  starting transfers between devices  19.1 us (4%)
  other arithmetic  18.6 us (4%)
  between operations  14.2 us (3%)
  blocking collectives  12.6 us (3%)
    all_to_all x1, waiting for transfers between devices, on_device(): lax.all_to_all(send_cot, 'sp', split_axis=0, concat_axis=0, tiled=True)  93.9 us
    all_to_all x1, waiting for transfers between devices, on_device(): lax.all_to_all(send_rows, 'sp', split_axis=0, concat_axis=0, tiled=True)  86.7 us
    reduce_scatter x1, waiting for transfers between devices, on_device(): lax.psum_scatter(partial_low, 'tp', scatter_dimension=2, tiled=True)  47 us
    reduce_scatter x1, waiting for transfers between devices, on_device(): lax.psum_scatter(lax.dot_general(resid_grad, conv_act, (((0,), (0,)), (()...  43.5 us
    all_to_all x1, waiting for transfers between devices, on_device(): lax.all_to_all(row_share.astype(jnp.bfloat16), 'sp', split_axis=0, concat...  28.3 us
  transfers between devices with their start and end apart: 7, of which 6 were waited for; matrix products, arithmetic and copies ran while one was open for 12% of the time, Pallas kernels for 0%

commit v1 on v0

--- a/solution.py
+++ b/solution.py
@@ -1,9 +1,280 @@
+import functools
+
 import jax
 import jax.numpy as jnp
 from jax import lax
+from jax.experimental import pallas as pl
+from jax.experimental.pallas import tpu as pltpu
 from jax.sharding import PartitionSpec as P
 
 norm_eps = 1e-06
+MESH = pl.DeviceIdType.MESH
+bf16 = jnp.bfloat16
+f32 = jnp.float32
+
+
+def doublings(count):
+    steps, step = [], 1
+    while step < count:
+        steps.append(step)
+        step *= 2
+    return steps
+
+
+def block_order(count):
+    low, high, order = 1, count - 1, []
+    while low <= high:
+        order.append(high)
+        if low < high:
+            order.append(low)
+        low, high = low + 1, high - 1
+    return order
+
+
+def greet(me_s, me_t, sp, tp):
+    barrier = pltpu.get_barrier_semaphore()
+    peers = [(me_s ^ d, me_t) for d in range(1, sp)] + [(me_s, me_t ^ m) for m in doublings(tp)]
+    for peer in peers:
+        pl.semaphore_signal(barrier, inc=1, device_id=peer, device_id_type=MESH)
+    pl.semaphore_wait(barrier, len(peers))
+
+
+def remote(source, target, send_sem, recv_sem, peer):
+    return pltpu.make_async_remote_copy(
+        src_ref=source,
+        dst_ref=target,
+        send_sem=send_sem,
+        recv_sem=recv_sem,
+        device_id=peer,
+        device_id_type=MESH,
+    )
+
+
+def dispatch_kernel(sp, tp, send_ref, out_ref, send_sem, recv_sem, own_sem):
+    me_s, me_t = lax.axis_index("sp"), lax.axis_index("tp")
+    share = send_ref.shape[-1]
+    steps = doublings(tp)
+    arrays = send_ref.shape[0]
+    events = [(a, d) for a in range(arrays) for d in [0] + block_order(sp)]
+
+    def cols(q):
+        return pl.ds(pl.multiple_of((me_t ^ q) * share, share), share)
+
+    greet(me_s, me_t, sp, tp)
+    copies = {}
+    for i, (a, d) in enumerate(events):
+        if d:
+            copies[0, i] = remote(
+                send_ref.at[a, me_s ^ d],
+                out_ref.at[a, me_s, :, cols(0)],
+                send_sem.at[0, i],
+                recv_sem.at[0, i],
+                (me_s ^ d, me_t),
+            )
+        else:
+            copies[0, i] = pltpu.make_async_copy(
+                send_ref.at[a, me_s], out_ref.at[a, me_s, :, cols(0)], own_sem.at[a]
+            )
+        copies[0, i].start()
+
+    def forward(i, q, m):
+        a, d = events[i]
+        place = out_ref.at[a, me_s ^ d, :, cols(q)]
+        source = send_ref.at[a, me_s] if d == 0 and q == 0 else place
+        copies[q ^ m, i] = remote(
+            source, place, send_sem.at[q ^ m, i], recv_sem.at[q ^ m, i], (me_s, me_t ^ m)
+        )
+        copies[q ^ m, i].start()
+
+    def relay(i):
+        for low in reversed(steps[1:]):
+            for q in range(low, tp, 2 * low):
+                copies[q, i].wait_recv()
+                for m in reversed(steps):
+                    if m < low:
+                        forward(i, q, m)
+
+    lag = 2
+    for i, (a, d) in enumerate(events):
+        if d:
+            copies[0, i].wait_recv()
+        for m in reversed(steps):
+            forward(i, 0, m)
+        if i >= lag:
+            relay(i - lag)
+    for i in range(max(0, len(events) - lag), len(events)):
+        relay(i)
+    for i, (a, d) in enumerate(events):
+        for q in range(1, tp, 2):
+            copies[q, i].wait_recv()
+        for q in range(tp):
+            if q or d:
+                copies[q, i].wait_send()
+            else:
+                copies[q, i].wait()
+
+
+def dispatch(send, sp, tp):
+    arrays, _, rows, share = send.shape
+    vmem = pl.BlockSpec(memory_space=pltpu.VMEM)
+    return pl.pallas_call(
+        functools.partial(dispatch_kernel, sp, tp),
+        out_shape=jax.ShapeDtypeStruct((arrays, sp, rows, share * tp), bf16),
+        in_specs=[vmem],
+        out_specs=vmem,
+        scratch_shapes=[
+            pltpu.SemaphoreType.DMA((tp, arrays * sp)),
+            pltpu.SemaphoreType.DMA((tp, arrays * sp)),
+            pltpu.SemaphoreType.DMA((arrays,)),
+        ],
+        compiler_params=pltpu.CompilerParams(collective_id=0, has_side_effects=True),
+    )(send)
+
+
+def return_kernel(
+    sp,
+    tp,
+    part_ref,
+    pick_ref,
+    cot_ref,
+    resid_ref,
+    got_ref,
+    sums_ref,
+    fin_ref,
+    back_ref,
+    acc_ref,
+    got_send,
+    got_recv,
+    back_send,
+    back_recv,
+    join_send,
+    join_recv,
+):
+    me_s, me_t = lax.axis_index("sp"), lax.axis_index("tp")
+    share = cot_ref.shape[-1]
+    steps = doublings(tp)
+    order = block_order(sp) + [0]
+    slot, sent_slot = {}, {}
+    for k, m in enumerate(steps):
+        for q in range(0, tp, 2 * m):
+            slot[k, q] = len(slot)
+            if k:
+                sent_slot[k, q ^ m] = len(sent_slot)
+
+    def cols(q):
+        return pl.ds(pl.multiple_of((me_t ^ q) * share, share), share)
+
+    greet(me_s, me_t, sp, tp)
+    copies = {}
+
+    def give(k, q, d, source):
+        m = steps[k]
+        place = slot[k, q ^ m]
+        copy = remote(
+            source,
+            got_ref.at[place, me_s ^ d],
+            got_send.at[place, d],
+            got_recv.at[place, d],
+            (me_s, me_t ^ m),
+        )
+        copy.start()
+        copies[k, q ^ m, d] = copy
+
+    for d in order:
+        for q in range(1, tp, 2):
+            give(0, q, d, part_ref.at[me_s ^ d, :, cols(q)])
+
+    def total(k, q, d):
+        value = part_ref[me_s ^ d, :, cols(q)].astype(f32)
+        for j in range(k):
+            value = value + got_ref[slot[j, q], me_s ^ d].astype(f32)
+        return value.astype(bf16)
+
+    def stage(k, d):
+        for q in range(0, tp, 2 * steps[k - 1]):
+            copies[k - 1, q, d].wait_recv()
+        if k < len(steps):
+            m = steps[k]
+            for q in range(m, tp, 2 * m):
+                held = sums_ref.at[sent_slot[k, q], me_s ^ d]
+                held[...] = total(k, q, d)
+                give(k, q, d, held)
+        elif d:
+            fin_ref[me_s ^ d] = total(k, 0, d)
+            copies["back", d] = remote(
+                fin_ref.at[me_s ^ d],
+                back_ref.at[me_s],
+                back_send.at[d],
+                back_recv.at[d],
+                (me_s ^ d, me_t),
+            )
+            copies["back", d].start()
+        else:
+            back_ref[me_s] = total(k, 0, d)
+
+    lag = 2
+    depth = len(steps)
+    for i in range(len(order) + lag * (depth - 1)):
+        for k in range(1, depth + 1):
+            at = i - lag * (k - 1)
+            if 0 <= at < len(order):
+                stage(k, order[at])
+
+    acc_ref[...] = cot_ref[...].astype(f32)
+    for d in [0] + order[:-1]:
+        if d:
+            copies["back", d].wait_recv()
+        acc_ref[...] += jnp.dot(
+            pick_ref[me_s ^ d], back_ref[me_s ^ d], preferred_element_type=f32
+        )
+    resid_ref[:, cols(0)] = acc_ref[...].astype(bf16)
+
+    def join(q, m):
+        place = resid_ref.at[:, cols(q)]
+        copies["join", q ^ m] = remote(
+            place, place, join_send.at[q ^ m], join_recv.at[q ^ m], (me_s, me_t ^ m)
+        )
+        copies["join", q ^ m].start()
+
+    for m in reversed(steps):
+        join(0, m)
+    for low in reversed(steps[1:]):
+        for q in range(low, tp, 2 * low):
+            copies["join", q].wait_recv()
+            for m in reversed(steps):
+                if m < low:
+                    join(q, m)
+    for q in range(1, tp, 2):
+        copies["join", q].wait_recv()
+    for copy in copies.values():
+        copy.wait_send()
+
+
+def give_back(part, picks, own_cot, sp, tp):
+    _, rows, width = part.shape
+    tok_rows, share = own_cot.shape
+    vmem = pl.BlockSpec(memory_space=pltpu.VMEM)
+    spare = max(1, tp // 2 - 1)
+    return pl.pallas_call(
+        functools.partial(return_kernel, sp, tp),
+        out_shape=jax.ShapeDtypeStruct((tok_rows, width), bf16),
+        in_specs=[vmem] * 3,
+        out_specs=vmem,
+        scratch_shapes=[
+            pltpu.VMEM((tp - 1, sp, rows, share), bf16),
+            pltpu.VMEM((spare, sp, rows, share), bf16),
+            pltpu.VMEM((sp, rows, share), bf16),
+            pltpu.VMEM((sp, rows, share), bf16),
+            pltpu.VMEM((tok_rows, share), f32),
+            pltpu.SemaphoreType.DMA((tp - 1, sp)),
+            pltpu.SemaphoreType.DMA((tp - 1, sp)),
+            pltpu.SemaphoreType.DMA((sp,)),
+            pltpu.SemaphoreType.DMA((sp,)),
+            pltpu.SemaphoreType.DMA((tp,)),
+            pltpu.SemaphoreType.DMA((tp,)),
+        ],
+        compiler_params=pltpu.CompilerParams(collective_id=1, has_side_effects=True),
+    )(part, picks, own_cot)
 
 
 def passed_along(value, axis, steps):
@@ -36,43 +307,49 @@
     local_exp = expert_gate.shape[0]
     experts = local_exp * sp_count
     capacity = 3 * top_count * tok_rows // (2 * experts)
-    assigns = tok_rows * top_count
-    flat_routes = routes.reshape(assigns)
-    onehot = (flat_routes[:, None] == jnp.arange(experts, dtype=jnp.int32)[None, :]).astype(
-        jnp.int32
-    )
-    slot_rank = jnp.sum((jnp.cumsum(onehot, axis=0) - onehot) * onehot, axis=1)
-    target = flat_routes * capacity + slot_rank
-    slot_ids = (
-        jnp.full((experts * capacity,), assigns, jnp.int32)
-        .at[target]
-        .set(jnp.arange(assigns, dtype=jnp.int32))
-    )
-    token_of = slot_ids // top_count
-    padded_in = jnp.concatenate([expert_input, jnp.zeros((1, model_width), jnp.bfloat16)], axis=0)
-    padded_cot = jnp.concatenate([cotangent, jnp.zeros((1, model_width), jnp.bfloat16)], axis=0)
-    padded_weight = jnp.concatenate(
-        [route_weight.reshape(assigns), jnp.zeros((1,), jnp.float32)], axis=0
-    )
-    send_rows = padded_in[token_of].reshape(experts, capacity, model_width)
-    send_cot = (padded_cot[token_of].astype(jnp.float32) * padded_weight[slot_ids][:, None]).astype(
-        jnp.bfloat16
-    )
-    send_cot = send_cot.reshape(experts, capacity, model_width)
-    got_rows, got_cot = (
-        lax.all_to_all(send_rows, "sp", split_axis=0, concat_axis=0, tiled=True),
-        lax.all_to_all(send_cot, "sp", split_axis=0, concat_axis=0, tiled=True),
-    )
-
-    def by_expert(arrived):
+    named = routes[:, :, None] == jnp.arange(experts, dtype=jnp.int32)
+    token_at = jnp.arange(tok_rows, dtype=jnp.int32)
+    earlier = (token_at[:, None] > token_at[None, :]).astype(jnp.bfloat16)
+    before = jnp.dot(
+        earlier, jnp.any(named, axis=1).astype(jnp.bfloat16), preferred_element_type=jnp.float32
+    )
+    slot_rank = jnp.sum(jnp.where(named, before[:, None, :], 0.0), axis=2).astype(jnp.int32)
+    target = routes * capacity + slot_rank
+    rows = local_exp * capacity
+    slot_at = (
+        jnp.arange(sp_count, dtype=jnp.int32)[:, None, None] * rows
+        + jnp.arange(rows, dtype=jnp.int32)[None, None, :]
+    )
+    pick = [
+        (target[:, k][None, :, None] == slot_at).astype(jnp.bfloat16) for k in range(top_count)
+    ]
+    picks = sum(pick[1:], pick[0])
+    share_at = lax.axis_index("tp") * share_cols
+    own_in = lax.dynamic_slice_in_dim(expert_input, share_at, share_cols, 1)
+    own_cot = lax.dynamic_slice_in_dim(cotangent, share_at, share_cols, 1)
+
+    def chosen(which, values):
+        return jnp.einsum("str,td->srd", which, values, preferred_element_type=jnp.float32)
+
+    send_rows = chosen(picks, own_in).astype(jnp.bfloat16)
+    send_cot = sum(
+        chosen(
+            pick[k],
+            (own_cot.astype(jnp.float32) * route_weight[:, k][:, None]).astype(jnp.bfloat16),
+        )
+        for k in range(top_count)
+    ).astype(jnp.bfloat16)
+    arrived = dispatch(jnp.stack([send_rows, send_cot]), sp_count, tp_count)
+
+    def by_expert(blocks):
         return (
-            arrived.reshape(sp_count, local_exp, capacity, model_width)
+            blocks.reshape(sp_count, local_exp, capacity, model_width)
             .transpose(1, 0, 2, 3)
             .reshape(local_exp, sp_count * capacity, model_width)
         )
 
-    slot_rows = by_expert(got_rows)
-    slot_cots = by_expert(got_cot)
+    slot_rows = by_expert(arrived[0])
+    slot_cots = by_expert(arrived[1])
     pre_gate = jnp.einsum(
         "lrd,ldf->lrf", slot_rows, expert_gate, preferred_element_type=jnp.float32
     )
@@ -99,20 +376,10 @@
     partial_src = (
         partial_rows.reshape(local_exp, sp_count, capacity, model_width)
         .transpose(1, 0, 2, 3)
-        .reshape(experts, capacity, model_width)
+        .reshape(sp_count, rows, model_width)
     )
     partial_low = partial_src.astype(jnp.bfloat16)
-    row_share = lax.psum_scatter(partial_low, "tp", scatter_dimension=2, tiled=True).astype(
-        jnp.float32
-    )
-    slot_back = lax.all_to_all(
-        row_share.astype(jnp.bfloat16), "sp", split_axis=0, concat_axis=0, tiled=True
-    )
-    picked = slot_back.reshape(experts * capacity, share_cols)[target].astype(jnp.float32)
-    combined = jnp.sum(picked.reshape(tok_rows, top_count, share_cols), axis=1)
-    own_cot = lax.dynamic_slice_in_dim(cotangent, lax.axis_index("tp") * share_cols, share_cols, 1)
-    resid_part = (own_cot.astype(jnp.float32) + combined).astype(jnp.bfloat16)
-    resid_grad = lax.all_gather(resid_part, "tp", axis=1, tiled=True)
+    resid_grad = give_back(partial_low, picks, own_cot, sp_count, tp_count)
     mix_grad = lax.dot_general(
         resid_grad, out_weight, (((1,), (1,)), ((), ())), preferred_element_type=jnp.float32
     )

time: 438 us -> 256 us (0.58)
  waiting for transfers between devices: 300 us -> 36.3 us
  Pallas kernels: 0 us -> 133 us
  local copies, waits for them, and re-layouts: 30.7 us -> 12.1 us
  starting transfers between devices: 19.1 us -> 1.59 us
  other arithmetic: 18.6 us -> 11.6 us
  matrix products: 41.8 us -> 34.8 us
    all_to_all x3 -> x0, waiting for transfers between devices: 209 us -> none  [the longest x1 93.9 us: on_device(): lax.all_to_all(send_cot, 'sp', split_axis=0, concat_axis=0, tiled=True)]
    pallas_call x0 -> x2, Pallas kernels: none -> 133 us  [the longest x1 80 us: dispatch(): pl.pallas_call(functools.partial(dispatch_kernel, sp, tp), out_shape=jax....]
    reduce_scatter x1 -> x0, waiting for transfers between devices: 47 us -> none  [on_device(): lax.psum_scatter(partial_low, 'tp', scatter_dimension=2, tiled=True)]
    gather x4 -> x0, local copies, waits for them, and re-layouts: 19.2 us -> none  [the longest x1 6.01 us: on_device(): send_rows = padded_in[token_of].reshape(experts, capacity, model_width)]
    all_to_all x3 -> x0, starting transfers between devices: 17.4 us -> none  [the longest x1 7.31 us: on_device(): lax.all_to_all(send_rows, 'sp', split_axis=0, concat_axis=0, tiled=True)]
    slice x2 -> x3, local copies, waits for them, and re-layouts: 0.21 us -> 8.43 us  [the longest x1 7.63 us: on_device(): slot_cots = by_expert(arrived[1])]
    convert_element_type x3 -> x0, other arithmetic: 7.39 us -> none  [the longest x1 5.43 us: on_device(): (padded_cot[token_of].astype(jnp.float32) * padded_weight[slot_ids][:, No...]
    reduce_scatter x1, waiting for transfers between devices: 43.5 us -> 36.3 us  [on_device(): lax.psum_scatter(lax.dot_general(resid_grad, conv_act, (((0,), (0,)), (()...]
  transfers between devices with their start and end apart: 7 -> 2, of which waited for: 6 -> 1; matrix products, arithmetic and copies ran while one was open for 12% -> 7% of each run, Pallas kernels for 0% -> 0%
where the time goes in v1:
time: 256 us; the launch traced here: 255 us
  Pallas kernels  133 us (52%)
  waiting for transfers between devices  36.3 us (14%)
  matrix products  34.8 us (14%)
  between operations  14.4 us (6%)
  local copies, waits for them, and re-layouts  12.1 us (5%)
  blocking collectives  11.9 us (5%)
  other arithmetic  11.6 us (5%)
    pallas_call x1, Pallas kernels, dispatch(): pl.pallas_call(functools.partial(dispatch_kernel, sp, tp), out_shape=jax....  80 us
    pallas_call x1, Pallas kernels, give_back(): pl.pallas_call(functools.partial(return_kernel, sp, tp), out_shape=jax.Sh...  52.7 us
    reduce_scatter x1, waiting for transfers between devices, on_device(): lax.psum_scatter(lax.dot_general(resid_grad, conv_act, (((0,), (0,)), (()...  36.3 us
    slice x1, local copies, waits for them, and re-layouts, on_device(): slot_cots = by_expert(arrived[1])  7.63 us
    psum x1, blocking collectives, on_device(): lax.psum((jnp.sum(conv_vals, axis=1), jnp.sum(conv_vals * conv_vals, axis...  6.23 us
    psum x1, blocking collectives, on_device(): lax.psum((jnp.sum(norm_grad, axis=1), jnp.sum(norm_grad * normed, axis=1)...  5.63 us
    dot_general x1, matrix products, on_device(): jnp.einsum('lrd,lrf->ldf', slot_rows, gate_pre, preferred_element_type=jn...  5.54 us
    dot_general x1, matrix products, on_device(): jnp.einsum('lrd,ldf->lrf', slot_rows, expert_gate, preferred_element_type...  5.48 us
  transfers between devices with their start and end apart: 2, of which 1 were waited for; matrix products, arithmetic and copies ran while one was open for 7% of the time, Pallas kernels for 0%

profile of v1, /device:TPU:0, one launch (start us, length us, event | category | flops | bytes accessed | tf_op | source)
XLA Modules:
  0.0 255.3 jit_solution(10249445945716418791)
XLA Ops:
  7.2 0.0 copy-start
  7.2 0.0 reduce-scatter.2.cloned.1.call-start
  7.2 0.1 iota_add_fusion
  7.3 0.8 fusion.153
  8.1 0.1 fusion.30
  8.2 0.8 select_reduce_fusion
  9.0 0.7 convert_add_fusion
  9.7 0.8 slice_reduce_fusion.3
  10.5 1.0 constant_dynamic-slice_fusion.cot_ref
  11.5 0.0 copy-start.1
  11.5 1.8 fusion.7.pick_ref
  13.3 0.0 copy-done
  13.3 1.0 fusion.12
  14.3 1.2 fusion.1
  15.5 0.0 copy-done.1
  15.5 1.2 fusion.13
  16.7 1.6 pad_maximum_fusion.send_ref
  18.3 80.0 %shard_map.189 = bf16[2,8,144,2048]{3,2,1,0:T(8,128)(2,1)} custom-call(bf16[2,8,144,512]{3,2,1,0:T(8,128)(2,1)} %pad_maximum_fusion.send_ref), custom_call_target="tpu_custom_call" | custom-call | tf_op jit(solution)/shard_map/pallas_call | solution.py:120
  98.4 0.0 copy-start.6
  98.4 7.6 %fusion.159 = (bf16[1,8,144,2048]{3,2,1,0:T(8,128)(2,1)S(1)}, bf16[1,8,144,2048]{3,2,1,0:T(8,128)(2,1)}) fusion(bf16[2,8,144,2048]{3,2,1,0:T(8,128)(2,1)} %shard_map.189), kind=kLoop, calls=%fused_computation.243 | loop fusion | bytes 18874368 | tf_op jit(solution)/shard_map/slice | solution.py:352
  106.0 0.0 copy-done.6
  106.0 5.5 %fusion.21 = f32[1152,256]{1,0:T(8,128)S(1)} fusion(bf16[1152,2048]{1,0:T(8,128)(2,1)} %bitcast.89, bf16[1,2048,256]{2,1,0:T(8,128)(2,1)S(1)} %copy-done.6), kind=kOutput, calls=%fused_computation.61 | convolution fusion | flops 1207959552 | bytes 6946816 | tf_op jit(solution)/shard_map/lrd,ldf->lrf/dot_general | solution.py:353
  111.5 0.0 copy-done.4
  111.5 0.3 copy-done.7
  111.8 1.4 fusion.24
  113.2 0.0 copy-start.19
  113.2 0.0 copy-done.3
  113.2 0.2 copy-done.14
  113.4 1.8 multiply_convert_fusion.1
  115.3 0.0 copy-start.5
  115.3 0.0 copy-start.9
  115.3 1.4 fusion.19
  116.8 0.2 convert_reduce_fusion
  116.9 0.0 copy-done.10
  117.0 3.7 %fusion = bf16[1152,2048]{1,0:T(8,128)(2,1)} fusion(f32[1152,2048]{1,0:T(8,128)S(1)} %fusion.19, bf16[1152,256]{1,0:T(8,128)(2,1)S(1)} %get-tuple-element.44, bf16[1,2048,256]{2,1,0:T(8,128)(2,1)S(1)} %copy-done.7), kind=kOutput, calls=%fused_computation.1 | convolution fusion | flops 1212678144 | bytes 15794176 | tf_op jit(solution)/shard_map/lrf,ldf->lrd/dot_general | solution.py:373
  120.7 52.7 %shard_map.190 = bf16[384,2048]{1,0:T(8,128)(2,1)} custom-call(bf16[8,144,2048]{2,1,0:T(8,128)(2,1)} %bitcast.84, bf16[8,384,144]{2,1,0:T(8,128)(2,1)} %fusion.7.pick_ref, bf16[384,512]{1,0:T(8,128)(2,1)} %copy-done.1), custom_call_target="tpu_custom_call" | custom-call | tf_op jit(solution)/shard_map/pallas_call | solution.py:258
  173.4 6.2 %all-reduce.1 = (f32[384]{0:T(512)S(1)}, f32[384]{0:T(512)S(1)}) all-reduce(f32[384]{0:T(512)S(1)} %get-tuple-element.31, f32[384]{0:T(512)S(1)} %get-tuple-element.30), channel_id=1, replica_groups=mesh['sp'=8,'tp'=4] {'tp'}, use_global_device_ids=true, to_apply=%region_5.6 | all-reduce | flops 768 | bytes 6144 | tf_op jit(solution)/shard_map/psum | solution.py:388
  179.6 0.0 copy-start.2
  179.6 3.4 %convolution_convert_fusion = bf16[2048,256]{1,0:T(8,128)(2,1)} fusion(bf16[384,2048]{1,0:T(8,128)(2,1)} %shard_map.190, bf16[384,256]{1,0:T(8,128)(2,1)S(1)} %copy-done.9, f32[256]{0:T(256)S(1)} %copy-done.15, f32[256]{0:T(256)S(1)} %copy-done.16, f32[384]{0:T(512)S(1)} %get-tuple-element.78, f32[384]{0:T(512)S(1)} %get-tuple-element.77), kind=kOutput, calls=%fused_computation.40 | convolution fusion | flops 404160512 | bytes 2823168 | tf_op jit(solution)/shard_map/dot_general | solution.py:418
  183.0 0.0 reduce-scatter.2.cloned.1.call-update
  183.1 2.6 %fusion.157 = (f32[384]{0:T(512)S(1)}, f32[384]{0:T(512)S(1)}, f32[384,256]{1,0:T(8,128)}) fusion(f32[384]{0:T(512)S(1)} %get-tuple-element.78, f32[384]{0:T(512)S(1)} %get-tuple-element.77, bf16[384,256]{1,0:T(8,128)(2,1)S(1)} %copy-done.9, f32[256]{0:T(256)S(1)} %copy-done.15, f32[256]{0:T(256)S(1)} %copy-done.16, bf16[384,2048]{1,0:T(8,128)(2,1)S(1)} %copy-done.2, ...), kind=kOutput, calls=%fused_computation.242 | convolution fusion | flops 404323584 | bytes 3219456 | tf_op jit(solution)/shard_map/dot_general | solution.py:383
  185.7 5.6 %all-reduce = (f32[384]{0:T(512)S(1)}, f32[384]{0:T(512)S(1)}) all-reduce(f32[384]{0:T(512)S(1)} %get-tuple-element.29, f32[384]{0:T(512)S(1)} %get-tuple-element.28), channel_id=1, replica_groups=mesh['sp'=8,'tp'=4] {'tp'}, use_global_device_ids=true, to_apply=%region_10.11 | all-reduce | flops 768 | bytes 6144 | tf_op jit(solution)/shard_map/psum | solution.py:399
  191.3 1.3 fusion.46
  192.6 0.0 slice-start.2
  192.6 0.0 copy-start.13
  192.6 0.0 slice-start.3
  192.6 0.0 copy-start.11
  192.6 1.6 collective-permute-start
  194.2 0.0 slice-start
  194.2 5.5 %convolution_bitcast_fusion.2 = f32[1,2048,256]{2,1,0:T(8,128)} fusion(bf16[1152,2048]{1,0:T(8,128)(2,1)} %bitcast.90, bf16[1152,256]{1,0:T(8,128)(2,1)} %copy-done.5), kind=kOutput, calls=%fused_computation.39 | convolution fusion | flops 1207959552 | bytes 7405568 | tf_op jit(solution)/shard_map/lrd,lrf->ldf/dot_general | solution.py:368
  199.8 0.0 copy-done.13
  199.8 0.0 copy-start.20
  199.8 2.9 %convolution_bitcast_fusion.1 = f32[1,2048,256]{2,1,0:T(8,128)} fusion(bf16[1152,2048]{1,0:T(8,128)(2,1)S(1)} %bitcast.94, bf16[1152,256]{1,0:T(8,128)(2,1)S(1)} %copy-done.11), kind=kOutput, calls=%fused_computation.38 | convolution fusion | flops 1207959552 | bytes 7405568 | tf_op jit(solution)/shard_map/lrd,lrf->ldf/dot_general | solution.py:369
  202.8 0.0 copy-done.18
  202.8 0.0 copy-start.8
  202.8 0.0 copy-start.12
  202.8 2.9 %convolution_bitcast_fusion = f32[1,256,2048]{2,1,0:T(8,128)} fusion(bf16[1152,2048]{1,0:T(8,128)(2,1)S(1)} %bitcast.88, f32[1152,256]{1,0:T(8,128)S(1)} %copy-done.20, f32[1152,256]{1,0:T(8,128)S(1)} %copy-done.18), kind=kOutput, calls=%fused_computation.37 | convolution fusion | flops 1209729024 | bytes 9175040 | tf_op jit(solution)/shard_map/lrf,lrd->lfd/dot_general | solution.py:363
  205.8 0.0 collective-permute-done
  205.8 2.7 %multiply_convert_fusion.4 = (bf16[384,256]{1,0:T(8,128)(2,1)}, f32[384,256]{1,0:T(8,128)S(1)}) fusion(bf16[384,256]{1,0:T(8,128)(2,1)S(1)} %copy-done.12, bf16[384,256]{1,0:T(8,128)(2,1)S(1)} %copy-done.8, f32[384,256]{1,0:T(8,128)S(1)} %fusion.46, f32[256]{0:T(256)S(1)} %bitcast.124, f32[30,256]{1,0:T(8,128)S(1)} %collective-permute-done, ...), kind=kLoop, calls=%fused_computation.212 | loop fusion | flops 9928704 | bytes 1438720 | tf_op jit(solution)/shard_map/convert_element_type | solution.py:416
  208.5 0.8 multiply_convert_fusion.5
  209.3 36.3 %reduce-scatter.2.cloned.1.call-done = bf16[256,256]{1,0:T(8,128)(2,1)} async-done(((bf16[2048,256]{1,0:T(8,128)(2,1)}), bf16[256,256]{1,0:T(8,128)(2,1)}) %reduce-scatter.2.cloned.1.call-update) | async-done | bytes 131088 | tf_op jit(solution)/shard_map/reduce_scatter | solution.py:417
  245.6 0.9 convert_bitcast_fusion
  246.5 0.8 copy.35
  247.4 1.1 copy.40
  (34 shorter events, 0.1 us)
Async XLA Ops:
  7.2 6.2 %copy-start = (bf16[384,2048]{1,0:T(8,128)(2,1)S(1)}, bf16[384,2048]{1,0:T(8,128)(2,1)}, u32[]{:S(2)}) copy-start(bf16[384,2048]{1,0:T(8,128)(2,1)} %param.14) | copy-start | bytes 4718596
  7.2 238.4 %reduce-scatter.2.cloned.1.call-start = ((), (), s32[]{:S(2)}) async-start(), calls=%async_computation.1 | async-start | bytes 1179648 | tf_op jit(solution)/shard_map/reduce_scatter | solution.py:417
  11.5 4.0 %copy-start.1 = (bf16[384,512]{1,0:T(8,128)(2,1)}, bf16[384,512]{1,0:T(8,128)(2,1)S(1)}, u32[]{:S(2)}) copy-start(bf16[384,512]{1,0:T(8,128)(2,1)S(1)} %constant_dynamic-slice_fusion.cot_ref) | copy-start | bytes 1179652
  98.4 7.6 %copy-start.6 = (bf16[1,2048,256]{2,1,0:T(8,128)(2,1)S(1)}, bf16[1,2048,256]{2,1,0:T(8,128)(2,1)}, u32[]{:S(2)}) copy-start(bf16[1,2048,256]{2,1,0:T(8,128)(2,1)} %param.18) | copy-start | bytes 3145732
  106.0 7.2 %copy-start.3 = (bf16[1,8,144,2048]{3,2,1,0:T(8,128)(2,1)}, bf16[1,8,144,2048]{3,2,1,0:T(8,128)(2,1)S(1)}, u32[]{:S(2)}) copy-start(bf16[1,8,144,2048]{3,2,1,0:T(8,128)(2,1)S(1)} %get-tuple-element.42) | copy-start | bytes 14155780
  106.0 5.5 %copy-start.4 = (bf16[1,8,144,2048]{3,2,1,0:T(8,128)(2,1)S(1)}, bf16[1,8,144,2048]{3,2,1,0:T(8,128)(2,1)}, u32[]{:S(2)}) copy-start(bf16[1,8,144,2048]{3,2,1,0:T(8,128)(2,1)} %get-tuple-element.43) | copy-start | bytes 14155780
  106.0 5.8 %copy-start.7 = (bf16[1,2048,256]{2,1,0:T(8,128)(2,1)S(1)}, bf16[1,2048,256]{2,1,0:T(8,128)(2,1)}, u32[]{:S(2)}) copy-start(bf16[1,2048,256]{2,1,0:T(8,128)(2,1)} %param.19) | copy-start | bytes 3145732
  111.8 1.4 copy-start.17
  111.8 1.7 copy-start.14
  113.2 2.1 copy-start.19
  115.3 1.5 copy-start.5
  115.3 1.7 copy-start.10
  115.3 1.5 copy-start.9
  120.7 58.9 %copy-start.15 = (f32[256]{0:T(256)S(1)}, f32[256]{0:T(256)}, u32[]{:S(2)}) copy-start(f32[256]{0:T(256)} %param.26) | copy-start | bytes 3076
  120.7 58.9 %copy-start.16 = (f32[256]{0:T(256)S(1)}, f32[256]{0:T(256)}, u32[]{:S(2)}) copy-start(f32[256]{0:T(256)} %param.25) | copy-start | bytes 3076
  179.6 3.4 %copy-start.2 = (bf16[384,2048]{1,0:T(8,128)(2,1)S(1)}, bf16[384,2048]{1,0:T(8,128)(2,1)}, u32[]{:S(2)}) copy-start(bf16[384,2048]{1,0:T(8,128)(2,1)} %shard_map.190) | copy-start | bytes 4718596
  192.6 7.2 %slice-start.2 = ((s8[4718592]{0:T(1024)(128)(4,1)}), s8[4194304]{0:T(1024)(128)(4,1)S(1)}, s32[]{:S(2)}) async-start(s8[4718592]{0:T(1024)(128)(4,1)} %bitcast.92), calls=%async_computation.4 | async-start | bytes 8388608
  192.6 7.2 %copy-start.13 = (f32[31,256]{1,0:T(8,128)S(1)}, f32[31,256]{1,0:T(8,128)}, u32[]{:S(2)}) copy-start(f32[31,256]{1,0:T(8,128)} %param.24) | copy-start | bytes 95236
  192.6 7.2 %slice-start.3 = ((s8[4718592]{0:T(1024)(128)(4,1)}), s8[524288]{0:T(1024)(128)(4,1)S(1)}, s32[]{:S(2)}) async-start(s8[4718592]{0:T(1024)(128)(4,1)} %bitcast.92), calls=%async_computation.5 | async-start | bytes 1048576
  192.6 7.2 %copy-start.11 = (bf16[1152,256]{1,0:T(8,128)(2,1)S(1)}, bf16[1152,256]{1,0:T(8,128)(2,1)}, u32[]{:S(2)}) copy-start(bf16[1152,256]{1,0:T(8,128)(2,1)} %copy-done.10) | copy-start | bytes 1769476
  192.6 13.1 %collective-permute-start = (f32[30,256]{1,0:T(8,128)S(1)}, f32[30,256]{1,0:T(8,128)S(1)}, u32[]{:S(2)}, u32[]{:S(2)}) collective-permute-start(f32[30,256]{1,0:T(8,128)S(1)} %slice.274), channel_id=1, source_target_pairs={{4,0},{8,4},{12,8},{16,12},{20,16},{24,20},{28,24},{5,1},{9,5},{13... | collective-permute-start | bytes 92168 | tf_op jit(solution)/shard_map/ppermute | solution.py:283
  194.2 8.6 %slice-start = ((s8[4718592]{0:T(1024)(128)(4,1)}), s8[4194304]{0:T(1024)(128)(4,1)S(1)}, s32[]{:S(2)}) async-start(s8[4718592]{0:T(1024)(128)(4,1)} %bitcast.86), calls=%async_computation.2 | async-start | bytes 8388608
  199.8 3.0 %slice-start.1 = ((s8[4718592]{0:T(1024)(128)(4,1)}), s8[524288]{0:T(1024)(128)(4,1)S(1)}, s32[]{:S(2)}) async-start(s8[4718592]{0:T(1024)(128)(4,1)} %bitcast.86), calls=%async_computation.3 | async-start | bytes 1048576
  199.8 3.0 %copy-start.18 = (f32[1152,256]{1,0:T(8,128)S(1)}, f32[1152,256]{1,0:T(8,128)}, u32[]{:S(2)}) copy-start(f32[1152,256]{1,0:T(8,128)} %copy-done.17) | copy-start | bytes 3538948
  199.8 3.0 %copy-start.20 = (f32[1152,256]{1,0:T(8,128)S(1)}, f32[1152,256]{1,0:T(8,128)}, u32[]{:S(2)}) copy-start(f32[1152,256]{1,0:T(8,128)} %copy-done.19) | copy-start | bytes 3538948
  202.8 3.0 %copy-start.8 = (bf16[384,256]{1,0:T(8,128)(2,1)S(1)}, bf16[384,256]{1,0:T(8,128)(2,1)}, u32[]{:S(2)}) copy-start(bf16[384,256]{1,0:T(8,128)(2,1)} %param.23) | copy-start | bytes 589828
  202.8 3.0 %copy-start.12 = (bf16[384,256]{1,0:T(8,128)(2,1)S(1)}, bf16[384,256]{1,0:T(8,128)(2,1)}, u32[]{:S(2)}) copy-start(bf16[384,256]{1,0:T(8,128)(2,1)} %param.22) | copy-start | bytes 589828
Sparse Core Ops, SparseCore 0:
  183.2 62.3 reduce-scatter.1

commit v2 on v1

v2 whole, which is shorter than its diff:
```python
import functools

import jax
import jax.numpy as jnp
from jax import lax
from jax.experimental import pallas as pl
from jax.experimental.pallas import tpu as pltpu
from jax.sharding import PartitionSpec as P

norm_eps = 1e-06
MESH = pl.DeviceIdType.MESH
bf16 = jnp.bfloat16
f32 = jnp.float32


def doublings(count):
    steps, step = [], 1
    while step < count:
        steps.append(step)
        step *= 2
    return steps


def block_order(count):
    low, high, order = 1, count - 1, []
    while low <= high:
        order.append(high)
        if low < high:
            order.append(low)
        low, high = low + 1, high - 1
    return order


def greet(me_s, me_t, sp, tp):
    barrier = pltpu.get_barrier_semaphore()
    peers = [(me_s ^ d, me_t) for d in range(1, sp)] + [(me_s, me_t ^ m) for m in doublings(tp)]
    for peer in peers:
        pl.semaphore_signal(barrier, inc=1, device_id=peer, device_id_type=MESH)
    pl.semaphore_wait(barrier, len(peers))


def remote(source, target, send_sem, recv_sem, peer):
    return pltpu.make_async_remote_copy(
        src_ref=source,
        dst_ref=target,
        send_sem=send_sem,
        recv_sem=recv_sem,
        device_id=peer,
        device_id_type=MESH,
    )


def expert_kernel(sp, tp, *refs):
    (rows_ref, cots_ref, gate_ref, up_ref, down_ref, pick_ref, cot_ref) = refs[:7]
    (resid_ref, gate_out, up_out, down_out) = refs[7:11]
    (in_ref, hid_ref, gpre_ref, upre_ref, part_ref, got_ref, sums_ref, fin_ref) = refs[11:19]
    (back_ref, acc_ref, own_sem, send_sem, recv_sem, got_send, got_recv) = refs[19:26]
    (back_send, back_recv, join_send, join_recv) = refs[26:]
    me_s, me_t = lax.axis_index("sp"), lax.axis_index("tp")
    share = cot_ref.shape[-1]
    local_exp, capacity = rows_ref.shape[1:3]
    steps = doublings(tp)
    depth = len(steps)
    order = [0] + block_order(sp)
    sent = (rows_ref, cots_ref)
    slot, sent_slot = {}, {}
    for k, m in enumerate(steps):
        for q in range(0, tp, 2 * m):
            slot[k, q] = len(slot)
            if k:
                sent_slot[k, q ^ m] = len(sent_slot)

    def cols(q):
        return pl.ds(pl.multiple_of((me_t ^ q) * share, share), share)

    greet(me_s, me_t, sp, tp)
    copies = {}

    for d in order:
        for a in range(2):
            if d:
                copy = remote(
                    sent[a].at[me_s ^ d],
                    in_ref.at[a, me_s, :, :, cols(0)],
                    send_sem.at[0, a, d],
                    recv_sem.at[0, a, d],
                    (me_s ^ d, me_t),
                )
            else:
                copy = pltpu.make_async_copy(
                    sent[a].at[me_s], in_ref.at[a, me_s, :, :, cols(0)], own_sem.at[a]
                )
            copy.start()
            copies[0, a, d] = copy

    def forward(a, d, q, m):
        place = in_ref.at[a, me_s ^ d, :, :, cols(q)]
        source = sent[a].at[me_s] if d == 0 and q == 0 else place
        copy = remote(
            source,
            place,
            send_sem.at[q ^ m, a, d],
            recv_sem.at[q ^ m, a, d],
            (me_s, me_t ^ m),
        )
        copy.start()
        copies[q ^ m, a, d] = copy

    def spread(d):
        for a in range(2):
            if d:
                copies[0, a, d].wait_recv()
            for m in reversed(steps):
                forward(a, d, 0, m)

    def relay(d):
        for a in range(2):
            for low in reversed(steps[1:]):
                for q in range(low, tp, 2 * low):
                    copies[q, a, d].wait_recv()
                    for m in reversed(steps):
                        if m < low:
                            forward(a, d, q, m)

    def give(k, q, d, source):
        m = steps[k]
        place = slot[k, q ^ m]
        copy = remote(
            source,
            got_ref.at[place, me_s ^ d],
            got_send.at[place, d],
            got_recv.at[place, d],
            (me_s, me_t ^ m),
        )
        copy.start()
        copies["got", k, q ^ m, d] = copy

    def dot(left, right, contract):
        return lax.dot_general(left, right, (contract, ((), ())), preferred_element_type=f32)

    def compute(d):
        for a in range(2):
            for q in range(1, tp, 2):
                copies[q, a, d].wait_recv()
            if d == 0:
                copies[0, a, d].wait()
        at = me_s ^ d
        for e in range(local_exp):
            slot_rows, slot_cots = in_ref[0, at, e], in_ref[1, at, e]
            pre_gate = dot(slot_rows, gate_ref[e], ((1,), (0,)))
            pre_up = dot(slot_rows, up_ref[e], ((1,), (0,)))
            hidden_grad = dot(slot_cots, down_ref[e], ((1,), (1,)))
            gate_sig = jax.nn.sigmoid(pre_gate)
            gate_act = pre_gate * gate_sig
            hid_ref[e, at] = (gate_act * pre_up).astype(bf16)
            gate_pre = (
                hidden_grad * pre_up * gate_sig * (1.0 + pre_gate * (1.0 - gate_sig))
            ).astype(bf16)
            up_pre = (hidden_grad * gate_act).astype(bf16)
            gpre_ref[e, at] = gate_pre
            upre_ref[e, at] = up_pre
            part = dot(gate_pre, gate_ref[e], ((1,), (1,)))
            part = part + dot(up_pre, up_ref[e], ((1,), (1,)))
            part_ref[at, e] = part.astype(bf16)
        for q in range(1, tp, 2):
            give(0, q, d, part_ref.at[at, :, :, cols(q)])

    def total(k, q, d):
        value = part_ref[me_s ^ d, :, :, cols(q)].astype(f32)
        for j in range(k):
            value = value + got_ref[slot[j, q], me_s ^ d].astype(f32)
        return value.astype(bf16)

    def reduce(k, d):
        for q in range(0, tp, 2 * steps[k - 1]):
            copies["got", k - 1, q, d].wait_recv()
        if k < depth:
            m = steps[k]
            for q in range(m, tp, 2 * m):
                held = sums_ref.at[sent_slot[k, q], me_s ^ d]
                held[...] = total(k, q, d)
                give(k, q, d, held)
        elif d:
            fin_ref[me_s ^ d] = total(k, 0, d)
            copy = remote(
                fin_ref.at[me_s ^ d],
                back_ref.at[me_s],
                back_send.at[d],
                back_recv.at[d],
                (me_s ^ d, me_t),
            )
            copy.start()
            copies["back", d] = copy
        else:
            back_ref[me_s] = total(k, 0, d)

    plan = [(0, spread), (1, relay), (2, compute)]
    plan += [(2 + k, functools.partial(reduce, k)) for k in range(1, depth + 1)]
    for i in range(len(order) + plan[-1][0]):
        for lag, act in plan:
            if 0 <= i - lag < len(order):
                act(order[i - lag])

    def weight_grad(e, left, right, out):
        if capacity % 16 == 0:
            whole = lambda value: value.reshape(sp * capacity, value.shape[-1])
            out[e] = dot(whole(left(slice(None))), whole(right(slice(None))), ((0,), (0,)))
        else:
            out[e] = jnp.zeros(out.shape[1:], f32)

            @pl.loop(0, sp)
            def _(at):
                out[e] += dot(left(at), right(at), ((0,), (0,)))

    for e in range(local_exp):
        weight_grad(e, lambda at: in_ref[0, at, e], lambda at: gpre_ref[e, at], gate_out)
        weight_grad(e, lambda at: in_ref[0, at, e], lambda at: upre_ref[e, at], up_out)
        weight_grad(e, lambda at: hid_ref[e, at], lambda at: in_ref[1, at, e], down_out)

    acc_ref[...] = cot_ref[...].astype(f32)
    for d in order:
        if d:
            copies["back", d].wait_recv()
        for e in range(local_exp):
            acc_ref[...] += dot(pick_ref[me_s ^ d, e], back_ref[me_s ^ d, e], ((1,), (0,)))
    resid_ref[:, cols(0)] = acc_ref[...].astype(bf16)

    def join(q, m):
        place = resid_ref.at[:, cols(q)]
        copy = remote(
            place, place, join_send.at[q ^ m], join_recv.at[q ^ m], (me_s, me_t ^ m)
        )
        copy.start()
        copies["join", q ^ m] = copy

    for m in reversed(steps):
        join(0, m)
    for low in reversed(steps[1:]):
        for q in range(low, tp, 2 * low):
            copies["join", q].wait_recv()
            for m in reversed(steps):
                if m < low:
                    join(q, m)
    for q in range(1, tp, 2):
        copies["join", q].wait_recv()
    for key, copy in copies.items():
        if not (key[0] == 0 and key[-1] == 0):
            copy.wait_send()


def run_experts(send_rows, send_cots, gate, up, down, picks, own_cot, sp, tp):
    _, local_exp, capacity, share = send_rows.shape
    width, hidden = gate.shape[1:]
    tok_rows = own_cot.shape[0]
    vmem = pl.BlockSpec(memory_space=pltpu.VMEM)
    spare = max(1, tp // 2 - 1)
    part = (sp, local_exp, capacity, share)
    kept = (local_exp, sp, capacity, hidden)
    dma = pltpu.SemaphoreType.DMA
    return pl.pallas_call(
        functools.partial(expert_kernel, sp, tp),
        out_shape=(
            jax.ShapeDtypeStruct((tok_rows, width), bf16),
            jax.ShapeDtypeStruct(gate.shape, f32),
            jax.ShapeDtypeStruct(up.shape, f32),
            jax.ShapeDtypeStruct(down.shape, f32),
        ),
        in_specs=[vmem] * 7,
        out_specs=(vmem,) * 4,
        scratch_shapes=[
            pltpu.VMEM((2, sp, local_exp, capacity, width), bf16),
            pltpu.VMEM(kept, bf16),
            pltpu.VMEM(kept, bf16),
            pltpu.VMEM(kept, bf16),
            pltpu.VMEM((sp, local_exp, capacity, width), bf16),
            pltpu.VMEM((tp - 1, *part), bf16),
            pltpu.VMEM((spare, *part), bf16),
            pltpu.VMEM(part, bf16),
            pltpu.VMEM(part, bf16),
            pltpu.VMEM((tok_rows, share), f32),
            dma((2,)),
            dma((tp, 2, sp)),
            dma((tp, 2, sp)),
            dma((tp - 1, sp)),
            dma((tp - 1, sp)),
            dma((sp,)),
            dma((sp,)),
            dma((tp,)),
            dma((tp,)),
        ],
        compiler_params=pltpu.CompilerParams(
            collective_id=0, has_side_effects=True, vmem_limit_bytes=62 * 1024 * 1024
        ),
    )(send_rows, send_cots, gate, up, down, picks, own_cot)


def passed_along(value, axis, steps):
    count = lax.axis_size(axis)
    leading, last = (max(0, -steps), min(count, count - steps))
    return lax.ppermute(value, axis, [(source, source + steps) for source in range(leading, last)])


def on_device(
    expert_input,
    cotangent,
    routes,
    route_weight,
    expert_gate,
    expert_up,
    expert_down,
    conv_out,
    conv_value,
    conv_gate,
    conv_taps,
    norm_gain,
    norm_bias,
    out_weight,
):
    sp_count = lax.axis_size("sp")
    tp_count = lax.axis_size("tp")
    tok_rows, model_width = expert_input.shape
    share_cols = model_width // tp_count
    top_count = routes.shape[1]
    local_exp = expert_gate.shape[0]
    experts = local_exp * sp_count
    capacity = 3 * top_count * tok_rows // (2 * experts)
    named = routes[:, :, None] == jnp.arange(experts, dtype=jnp.int32)
    token_at = jnp.arange(tok_rows, dtype=jnp.int32)
    earlier = (token_at[:, None] > token_at[None, :]).astype(jnp.bfloat16)
    before = jnp.dot(
        earlier, jnp.any(named, axis=1).astype(jnp.bfloat16), preferred_element_type=jnp.float32
    )
    slot_rank = jnp.sum(jnp.where(named, before[:, None, :], 0.0), axis=2).astype(jnp.int32)
    target = routes * capacity + slot_rank
    blocks = (sp_count, local_exp, tok_rows, capacity)
    slot_at = (
        lax.broadcasted_iota(jnp.int32, blocks, 0) * local_exp
        + lax.broadcasted_iota(jnp.int32, blocks, 1)
    ) * capacity + lax.broadcasted_iota(jnp.int32, blocks, 3)
    pick = [
        (target[:, k][None, None, :, None] == slot_at).astype(jnp.bfloat16) for k in range(top_count)
    ]
    picks = sum(pick[1:], pick[0])
    share_at = lax.axis_index("tp") * share_cols
    own_in = lax.dynamic_slice_in_dim(expert_input, share_at, share_cols, 1)
    own_cot = lax.dynamic_slice_in_dim(cotangent, share_at, share_cols, 1)

    def chosen(which, values):
        return jnp.einsum("setr,td->serd", which, values, preferred_element_type=jnp.float32)

    send_rows = chosen(picks, own_in).astype(jnp.bfloat16)
    send_cot = sum(
        chosen(
            pick[k],
            (own_cot.astype(jnp.float32) * route_weight[:, k][:, None]).astype(jnp.bfloat16),
        )
        for k in range(top_count)
    ).astype(jnp.bfloat16)
    resid_grad, gate_grad, up_grad, down_grad = run_experts(
        send_rows,
        send_cot,
        expert_gate,
        expert_up,
        expert_down,
        picks,
        own_cot,
        sp_count,
        tp_count,
    )
    mix_grad = lax.dot_general(
        resid_grad, out_weight, (((1,), (1,)), ((), ())), preferred_element_type=jnp.float32
    )
    channels = conv_out.shape[1] * tp_count
    conv_vals = conv_out.astype(jnp.float32)
    row_sum, row_square = lax.psum(
        (jnp.sum(conv_vals, axis=1), jnp.sum(conv_vals * conv_vals, axis=1)), "tp"
    )
    row_mean = (row_sum / channels)[:, None]
    row_var = (row_square / channels)[:, None] - row_mean * row_mean
    row_rstd = lax.rsqrt(row_var + norm_eps)
    normed = (conv_vals - row_mean) * row_rstd
    norm_pre = normed * norm_gain[None, :] + norm_bias[None, :]
    norm_sig = jax.nn.sigmoid(norm_pre)
    conv_act = (norm_pre * norm_sig).astype(jnp.bfloat16)
    norm_grad = mix_grad * norm_sig * (1.0 + norm_pre * (1.0 - norm_sig)) * norm_gain[None, :]
    grad_sum, grad_dot = lax.psum(
        (jnp.sum(norm_grad, axis=1), jnp.sum(norm_grad * normed, axis=1)), "tp"
    )
    conv_grad = row_rstd * (
        norm_grad - (grad_sum / channels)[:, None] - normed * (grad_dot / channels)[:, None]
    )
    taps_count = conv_taps.shape[0]
    next_rows = passed_along(conv_grad[: taps_count - 1], "sp", -1)
    extended = jnp.concatenate([conv_grad, next_rows], axis=0)
    glu_grad = jnp.zeros_like(conv_grad)
    for lag_index in range(taps_count):
        begin = taps_count - 1 - lag_index
        glu_grad = glu_grad + conv_taps[lag_index][None, :] * extended[begin : begin + tok_rows]
    gate_sig_in = jax.nn.sigmoid(conv_gate.astype(jnp.float32))
    value_grad = (glu_grad * gate_sig_in).astype(jnp.bfloat16)
    gate_in_grad = (
        glu_grad * conv_value.astype(jnp.float32) * gate_sig_in * (1.0 - gate_sig_in)
    ).astype(jnp.bfloat16)
    projected = lax.psum_scatter(
        lax.dot_general(
            resid_grad, conv_act, (((0,), (0,)), ((), ())), preferred_element_type=jnp.float32
        ).astype(jnp.bfloat16),
        "sp",
        scatter_dimension=0,
        tiled=True,
    ).astype(jnp.float32)
    out_weight_grad = projected.T
    return (gate_grad, up_grad, down_grad, resid_grad, out_weight_grad, value_grad, gate_in_grad)


def solution(mesh):
    return jax.shard_map(
        on_device,
        mesh=mesh,
        in_specs=(
            P("sp", None),
            P("sp", None),
            P("sp", None),
            P("sp", None),
            P("sp", None, "tp"),
            P("sp", None, "tp"),
            P("sp", "tp", None),
            P("sp", "tp"),
            P("sp", "tp"),
            P("sp", "tp"),
            P(None, "tp"),
            P("tp"),
            P("tp"),
            P("tp", None),
        ),
        out_specs=(
            P("sp", None, "tp"),
            P("sp", None, "tp"),
            P("sp", "tp", None),
            P("sp", None),
            P("tp", "sp"),
            P("sp", "tp"),
            P("sp", "tp"),
        ),
        check_vma=False,
    )
```

time: 256 us -> 230 us (0.90)
  matrix products: 34.8 us -> 10.8 us
  Pallas kernels: 133 us -> 119 us
  waiting for transfers between devices: 36.3 us -> 45 us
  blocking collectives: 11.9 us -> 15.1 us
    dot_general x11 -> x3, matrix products: 28.6 us -> 4.61 us  [chosen(): jnp.einsum('setr,td->serd', which, values, preferred_element_type=jnp.flo...]
    pallas_call x2 -> x1, Pallas kernels: 133 us -> 119 us  [run_experts(): pl.pallas_call(functools.partial(expert_kernel, sp, tp), out_shape=(jax.S...]
    slice x2 -> x1, local copies, waits for them, and re-layouts: 7.65 us -> 0.02 us  [on_device(): target[:, k][None, None, :, None] == slot_at]
    unnamed x52 -> x23, local copies, waits for them, and re-layouts: 2.57 us -> 8.88 us
    reduce_scatter x1, waiting for transfers between devices: 36.3 us -> 42.5 us  [on_device(): lax.psum_scatter(lax.dot_general(resid_grad, conv_act, (((0,), (0,)), (()...]
  transfers between devices with their start and end apart: 2 -> 2, of which waited for: 1 -> 2; matrix products, arithmetic and copies ran while one was open for 7% -> 5% of each run, Pallas kernels for 0% -> 0%
where the time goes in v2:
time: 230 us; the launch traced here: 229 us
  Pallas kernels  119 us (52%)
  waiting for transfers between devices  45 us (20%)
  blocking collectives  15.1 us (7%)
  between operations  14.2 us (6%)
  local copies, waits for them, and re-layouts  12.7 us (6%)
  other arithmetic  11.5 us (5%)
  matrix products  10.8 us (5%)
    pallas_call x1, Pallas kernels, run_experts(): pl.pallas_call(functools.partial(expert_kernel, sp, tp), out_shape=(jax.S...  119 us
    reduce_scatter x1, waiting for transfers between devices, on_device(): lax.psum_scatter(lax.dot_general(resid_grad, conv_act, (((0,), (0,)), (()...  42.5 us
    unnamed x23, local copies, waits for them, and re-layouts  8.88 us
    psum x1, blocking collectives, on_device(): lax.psum((jnp.sum(conv_vals, axis=1), jnp.sum(conv_vals * conv_vals, axis...  8.33 us
    psum x1, blocking collectives, on_device(): lax.psum((jnp.sum(norm_grad, axis=1), jnp.sum(norm_grad * normed, axis=1)...  6.72 us
    dot_general x3, matrix products, chosen(): jnp.einsum('setr,td->serd', which, values, preferred_element_type=jnp.flo...  4.61 us
  transfers between devices with their start and end apart: 2, of which 2 were waited for; matrix products, arithmetic and copies ran while one was open for 5% of the time, Pallas kernels for 0%

profile of v2, /device:TPU:0, one launch (start us, length us, event | category | flops | bytes accessed | tf_op | source)
XLA Modules:
  0.0 229.3 jit_solution(9695490843629529576)
XLA Ops:
  7.2 0.0 copy-start
  7.2 0.0 reduce-scatter.2.cloned.1.call-start
  7.2 0.8 fusion.154
  8.0 0.1 fusion.33
  8.2 0.8 select_reduce_fusion
  8.9 0.7 convert_add_fusion
  9.7 0.8 slice_reduce_fusion.2
  10.4 1.0 constant_dynamic-slice_fusion.refs_6_
  11.5 0.0 copy-start.1
  11.5 1.8 fusion.12.refs_5_
  13.3 0.0 copy-done
  13.3 0.0 copy-start.6
  13.3 1.9 fusion.15.refs_0_
  15.1 0.0 copy-done.6
  15.1 0.2 convert_reduce_fusion
  15.3 0.9 fusion.6
  16.2 0.0 copy-done.1
  16.2 1.9 fusion.16.refs_1_
  18.1 8.3 %all-reduce.1 = (f32[384]{0:T(512)S(1)}, f32[384]{0:T(512)S(1)}) all-reduce(f32[384]{0:T(512)S(1)} %get-tuple-element.32, f32[384]{0:T(512)S(1)} %get-tuple-element.31), channel_id=1, replica_groups=mesh['sp'=8,'tp'=4] {'tp'}, use_global_device_ids=true, to_apply=%region_5.6 | all-reduce | flops 768 | bytes 6144 | tf_op jit(solution)/shard_map/psum | solution.py:375
  26.4 0.0 copy-start.7
  26.4 0.0 copy-start.8
  26.4 118.7 %shard_map.189 = (bf16[384,2048]{1,0:T(8,128)(2,1)}, f32[1,2048,256]{2,1,0:T(8,128)}, f32[1,2048,256]{2,1,0:T(8,128)}, f32[1,256,2048]{2,1,0:T(8,128)}) custom-call(bf16[8,1,144,512]{3,2,1,0:T(8,128)(2,1)} %fusion.15.refs_0_, bf16[8,1,144,512]{3,2,1,0:T(8,128)(2,1)} %fusion.16.refs_1_, bf16[1,2048,256]{2,1,0:T(8,128)(2,1)} %refs_2_.1, ...), custom_call_target="tpu_custom_call" | custom-call | tf_op jit(solution)/shard_map/pallas_call | solution.py:260
  145.2 0.0 copy-done.7
  145.2 0.0 copy-done.8
  145.2 0.0 copy-start.4
  145.2 3.4 %convolution_convert_fusion = bf16[2048,256]{1,0:T(8,128)(2,1)} fusion(bf16[384,2048]{1,0:T(8,128)(2,1)} %get-tuple-element.89, bf16[384,256]{1,0:T(8,128)(2,1)S(1)} %copy-done.6, f32[256]{0:T(256)S(1)} %copy-done.7, f32[256]{0:T(256)S(1)} %copy-done.8, f32[384]{0:T(512)S(1)} %get-tuple-element.75, f32[384]{0:T(512)S(1)} %get-tuple-element.74), kind=kOutput, calls=%fused_computation.34 | convolution fusion | flops 404160512 | bytes 2823168 | tf_op jit(solution)/shard_map/dot_general | solution.py:405
  148.6 0.0 reduce-scatter.2.cloned.1.call-update
  148.6 0.0 copy-done.4
  148.6 0.0 copy-start.5
  148.6 2.7 %fusion.157 = (f32[384]{0:T(512)S(1)}, f32[384]{0:T(512)S(1)}, f32[384,256]{1,0:T(8,128)}) fusion(f32[384]{0:T(512)S(1)} %get-tuple-element.75, f32[384]{0:T(512)S(1)} %get-tuple-element.74, bf16[384,256]{1,0:T(8,128)(2,1)S(1)} %copy-done.6, f32[256]{0:T(256)} %param.26, f32[256]{0:T(256)} %param.25, bf16[384,2048]{1,0:T(8,128)(2,1)S(1)} %copy-done.4, ...), kind=kOutput, calls=%fused_computation.230 | convolution fusion | flops 404323584 | bytes 3219456 | tf_op jit(solution)/shard_map/dot_general | solution.py:370
  151.3 6.7 %all-reduce = (f32[384]{0:T(512)}, f32[384]{0:T(512)}) all-reduce(f32[384]{0:T(512)S(1)} %get-tuple-element.30, f32[384]{0:T(512)S(1)} %get-tuple-element.29), channel_id=1, replica_groups=mesh['sp'=8,'tp'=4] {'tp'}, use_global_device_ids=true, to_apply=%region_10.11 | all-reduce | flops 768 | bytes 6144 | tf_op jit(solution)/shard_map/psum | solution.py:386
  158.0 0.7 broadcast_multiply_fusion
  158.7 1.3 fusion.49
  160.0 1.3 collective-permute-start
  161.3 1.0 fusion.159
  162.4 1.0 fusion.160
  163.3 2.5 %collective-permute-done = f32[30,256]{1,0:T(8,128)S(1)} collective-permute-done((f32[30,256]{1,0:T(8,128)S(1)}, f32[30,256]{1,0:T(8,128)S(1)}, u32[]{:S(2)}, u32[]{:S(2)}) %collective-permute-start) | collective-permute-done | bytes 30752 | tf_op jit(solution)/shard_map/ppermute | solution.py:300
  165.8 0.0 copy-done.5
  165.8 3.6 %multiply_convert_fusion = (bf16[384,256]{1,0:T(8,128)(2,1)}, f32[384,256]{1,0:T(8,128)S(1)}) fusion(bf16[384,256]{1,0:T(8,128)(2,1)} %param.22, bf16[384,256]{1,0:T(8,128)(2,1)S(1)} %copy-done.5, f32[384,256]{1,0:T(8,128)S(1)} %fusion.49, f32[256]{0:T(256)S(1)} %bitcast.79, f32[30,256]{1,0:T(8,128)S(1)} %collective-permute-done, f32[256]{0:T(256)S(1)} %bitcast.80, ...), kind=kLoop, calls=%fused_computation.202 | loop fusion | flops 9928704 | bytes 1438720 | tf_op jit(solution)/shard_map/convert_element_type | solution.py:403
  169.4 0.8 multiply_convert_fusion.1
  170.2 42.5 %reduce-scatter.2.cloned.1.call-done = bf16[256,256]{1,0:T(8,128)(2,1)} async-done(((bf16[2048,256]{1,0:T(8,128)(2,1)}), bf16[256,256]{1,0:T(8,128)(2,1)}) %reduce-scatter.2.cloned.1.call-update) | async-done | bytes 131088 | tf_op jit(solution)/shard_map/reduce_scatter | solution.py:404
  212.7 0.9 convert_bitcast_fusion
  213.6 0.8 copy.24
  214.4 0.0 copy-start.3
  214.4 3.2 %copy.29 = f32[1,2048,256]{2,1,0:T(8,128)} copy(f32[1,2048,256]{2,1,0:T(8,128)} %get-tuple-element.86) | data formatting | bytes 4194304
  217.6 0.0 copy-done.3
  217.6 0.0 copy-start.2
  217.6 1.3 copy.30
  219.0 1.0 copy-done.2
  220.0 1.3 copy.31
  221.3 1.1 copy.32
  (4 shorter events, 0.0 us)
Async XLA Ops:
  7.2 6.1 %copy-start = (bf16[384,2048]{1,0:T(8,128)(2,1)S(1)}, bf16[384,2048]{1,0:T(8,128)(2,1)}, u32[]{:S(2)}) copy-start(bf16[384,2048]{1,0:T(8,128)(2,1)} %param.14) | copy-start | bytes 4718596
  7.2 205.5 %reduce-scatter.2.cloned.1.call-start = ((), (), s32[]{:S(2)}) async-start(), calls=%async_computation.1 | async-start | bytes 1179648 | tf_op jit(solution)/shard_map/reduce_scatter | solution.py:404
  11.5 4.7 %copy-start.1 = (bf16[384,512]{1,0:T(8,128)(2,1)}, bf16[384,512]{1,0:T(8,128)(2,1)S(1)}, u32[]{:S(2)}) copy-start(bf16[384,512]{1,0:T(8,128)(2,1)S(1)} %constant_dynamic-slice_fusion.refs_6_) | copy-start | bytes 1179652
  13.3 1.9 copy-start.6
  26.4 118.7 %copy-start.7 = (f32[256]{0:T(256)S(1)}, f32[256]{0:T(256)}, u32[]{:S(2)}) copy-start(f32[256]{0:T(256)} %param.26) | copy-start | bytes 3076
  26.4 118.7 %copy-start.8 = (f32[256]{0:T(256)S(1)}, f32[256]{0:T(256)}, u32[]{:S(2)}) copy-start(f32[256]{0:T(256)} %param.25) | copy-start | bytes 3076
  145.2 3.4 %copy-start.4 = (bf16[384,2048]{1,0:T(8,128)(2,1)S(1)}, bf16[384,2048]{1,0:T(8,128)(2,1)}, u32[]{:S(2)}) copy-start(bf16[384,2048]{1,0:T(8,128)(2,1)} %get-tuple-element.89) | copy-start | bytes 4718596
  148.6 17.2 %copy-start.5 = (bf16[384,256]{1,0:T(8,128)(2,1)S(1)}, bf16[384,256]{1,0:T(8,128)(2,1)}, u32[]{:S(2)}) copy-start(bf16[384,256]{1,0:T(8,128)(2,1)} %param.23) | copy-start | bytes 589828
  160.0 5.8 %collective-permute-start = (f32[30,256]{1,0:T(8,128)S(1)}, f32[30,256]{1,0:T(8,128)S(1)}, u32[]{:S(2)}, u32[]{:S(2)}) collective-permute-start(f32[30,256]{1,0:T(8,128)S(1)} %slice.266), channel_id=1, source_target_pairs={{4,0},{8,4},{12,8},{16,12},{20,16},{24,20},{28,24},{5,1},{9,5},{13... | collective-permute-start | bytes 92168 | tf_op jit(solution)/shard_map/ppermute | solution.py:300
  214.4 3.2 %copy-start.3 = (f32[1,2048,256]{2,1,0:T(8,128)S(1)}, f32[1,2048,256]{2,1,0:T(8,128)}, u32[]{:S(2)}) copy-start(f32[1,2048,256]{2,1,0:T(8,128)} %get-tuple-element.87) | copy-start | bytes 6291460
  217.6 2.3 %copy-start.2 = (f32[1,256,2048]{2,1,0:T(8,128)S(1)}, f32[1,256,2048]{2,1,0:T(8,128)}, u32[]{:S(2)}) copy-start(f32[1,256,2048]{2,1,0:T(8,128)} %get-tuple-element.88) | copy-start | bytes 6291460
Sparse Core Ops, SparseCore 0:
  148.7 63.8 reduce-scatter.1

commit v3 on v2

--- a/solution.py
+++ b/solution.py
@@ -33,7 +33,7 @@
 
 def greet(me_s, me_t, sp, tp):
     barrier = pltpu.get_barrier_semaphore()
-    peers = [(me_s ^ d, me_t) for d in range(1, sp)] + [(me_s, me_t ^ m) for m in doublings(tp)]
+    peers = [(me_s ^ d, me_t) for d in range(1, sp)] + [(me_s, me_t ^ q) for q in range(1, tp)]
     for peer in peers:
         pl.semaphore_signal(barrier, inc=1, device_id=peer, device_id_type=MESH)
     pl.semaphore_wait(barrier, len(peers))
@@ -50,12 +50,39 @@
     )
 
 
+def two_rows(first, second):
+    lane = lax.broadcasted_iota(jnp.int32, (first.shape[0], 128), 1)
+    tile = jnp.where(lane == 0, first, jnp.where(lane == 1, second, 0.0))
+    return tile.T[:8]
+
+
+def share_sums(held_ref, send_sem, recv_sem, me_s, me_t, tp):
+    copies = [
+        remote(
+            held_ref.at[0], held_ref.at[q], send_sem.at[q], recv_sem.at[q], (me_s, me_t ^ q)
+        )
+        for q in range(1, tp)
+    ]
+    for copy in copies:
+        copy.start()
+    return copies
+
+
+def summed(held_ref, copies):
+    value = held_ref[0]
+    for q, copy in enumerate(copies, 1):
+        copy.wait_recv()
+        value = value + held_ref[q]
+    return value
+
+
 def expert_kernel(sp, tp, *refs):
-    (rows_ref, cots_ref, gate_ref, up_ref, down_ref, pick_ref, cot_ref) = refs[:7]
-    (resid_ref, gate_out, up_out, down_out) = refs[7:11]
+    (rows_ref, cots_ref, gate_ref, up_ref, down_ref, pick_ref, cot_ref, conv_ref) = refs[:8]
+    (resid_ref, gate_out, up_out, down_out, stats_out) = refs[8:13]
+    refs = refs[2:]
     (in_ref, hid_ref, gpre_ref, upre_ref, part_ref, got_ref, sums_ref, fin_ref) = refs[11:19]
     (back_ref, acc_ref, own_sem, send_sem, recv_sem, got_send, got_recv) = refs[19:26]
-    (back_send, back_recv, join_send, join_recv) = refs[26:]
+    (back_send, back_recv, join_send, join_recv, stat_ref, stat_send, stat_recv) = refs[26:]
     me_s, me_t = lax.axis_index("sp"), lax.axis_index("tp")
     share = cot_ref.shape[-1]
     local_exp, capacity = rows_ref.shape[1:3]
@@ -194,9 +221,18 @@
         else:
             back_ref[me_s] = total(k, 0, d)
 
+    conv_vals = conv_ref[...].astype(f32)
+    stat_ref[0] = two_rows(
+        jnp.sum(conv_vals, axis=1, keepdims=True),
+        jnp.sum(conv_vals * conv_vals, axis=1, keepdims=True),
+    )
+
     plan = [(0, spread), (1, relay), (2, compute)]
     plan += [(2 + k, functools.partial(reduce, k)) for k in range(1, depth + 1)]
+    stat_copies = []
     for i in range(len(order) + plan[-1][0]):
+        if i == 1:
+            stat_copies = share_sums(stat_ref, stat_send, stat_recv, me_s, me_t, tp)
         for lag, act in plan:
             if 0 <= i - lag < len(order):
                 act(order[i - lag])
@@ -243,12 +279,15 @@
                     join(q, m)
     for q in range(1, tp, 2):
         copies["join", q].wait_recv()
+    stats_out[...] = summed(stat_ref, stat_copies)
+    for copy in stat_copies:
+        copy.wait_send()
     for key, copy in copies.items():
         if not (key[0] == 0 and key[-1] == 0):
             copy.wait_send()
 
 
-def run_experts(send_rows, send_cots, gate, up, down, picks, own_cot, sp, tp):
+def run_experts(send_rows, send_cots, gate, up, down, picks, own_cot, conv_out, sp, tp):
     _, local_exp, capacity, share = send_rows.shape
     width, hidden = gate.shape[1:]
     tok_rows = own_cot.shape[0]
@@ -264,9 +303,10 @@
             jax.ShapeDtypeStruct(gate.shape, f32),
             jax.ShapeDtypeStruct(up.shape, f32),
             jax.ShapeDtypeStruct(down.shape, f32),
+            jax.ShapeDtypeStruct((8, tok_rows), f32),
         ),
-        in_specs=[vmem] * 7,
-        out_specs=(vmem,) * 4,
+        in_specs=[vmem] * 8,
+        out_specs=(vmem,) * 5,
         scratch_shapes=[
             pltpu.VMEM((2, sp, local_exp, capacity, width), bf16),
             pltpu.VMEM(kept, bf16),
@@ -287,17 +327,168 @@
             dma((sp,)),
             dma((tp,)),
             dma((tp,)),
+            pltpu.VMEM((tp, 8, tok_rows), f32),
+            dma((tp,)),
+            dma((tp,)),
         ],
         compiler_params=pltpu.CompilerParams(
             collective_id=0, has_side_effects=True, vmem_limit_bytes=62 * 1024 * 1024
         ),
-    )(send_rows, send_cots, gate, up, down, picks, own_cot)
-
-
-def passed_along(value, axis, steps):
-    count = lax.axis_size(axis)
-    leading, last = (max(0, -steps), min(count, count - steps))
-    return lax.ppermute(value, axis, [(source, source + steps) for source in range(leading, last)])
+    )(send_rows, send_cots, gate, up, down, picks, own_cot, conv_out)
+
+
+def conv_kernel(sp, tp, *refs):
+    (resid_ref, stats_ref, conv_ref, value_ref, gate_ref, taps_ref) = refs[:6]
+    (gain_ref, bias_ref, weight_ref) = refs[6:9]
+    (weight_out, value_out, gate_out) = refs[9:12]
+    (proj_ref, low_ref, near_ref, sum_ref, far_ref, ext_ref, halo_ref, stat_ref) = refs[12:20]
+    (near_send, near_recv, far_send, far_recv) = refs[20:24]
+    (halo_send, halo_recv, stat_send, stat_recv) = refs[24:]
+    me_s, me_t = lax.axis_index("sp"), lax.axis_index("tp")
+    tok_rows, own_channels = conv_ref.shape
+    channels = own_channels * tp
+    taps_count = taps_ref.shape[0]
+    halo_rows = halo_ref.shape[0]
+    pairs = min(2, sp)
+    order = [d for d in block_order(sp) if d % pairs == 0] + [0]
+
+    greet(me_s, me_t, sp, tp)
+
+    totals = stats_ref[...].T / channels
+    row_mean = totals[:, 0:1]
+    row_rstd = lax.rsqrt(totals[:, 1:2] - row_mean * row_mean + norm_eps)
+    normed = (conv_ref[...].astype(f32) - row_mean) * row_rstd
+    norm_pre = normed * gain_ref[...] + bias_ref[...]
+    norm_sig = jax.nn.sigmoid(norm_pre)
+    conv_act = (norm_pre * norm_sig).astype(bf16)
+    projected = lax.dot_general(
+        resid_ref[...], conv_act, (((0,), (0,)), ((), ())), preferred_element_type=f32
+    )
+    proj_ref[...] = projected.reshape(proj_ref.shape)
+    low_ref[...] = proj_ref[...].astype(bf16)
+
+    near, far = {}, {}
+    if pairs == 2:
+        for d in order:
+            near[d] = remote(
+                low_ref.at[me_s ^ 1 ^ d],
+                near_ref.at[d // 2],
+                near_send.at[d // 2],
+                near_recv.at[d // 2],
+                (me_s ^ 1, me_t),
+            )
+            near[d].start()
+
+    def pass_on(d):
+        near[d].wait_recv()
+        if d:
+            sum_ref[d // 2] = (proj_ref[me_s ^ d] + near_ref[d // 2].astype(f32)).astype(bf16)
+            far[d] = remote(
+                sum_ref.at[d // 2],
+                far_ref.at[d // 2],
+                far_send.at[d // 2],
+                far_recv.at[d // 2],
+                (me_s ^ d, me_t),
+            )
+            far[d].start()
+
+    mix_grad = lax.dot_general(
+        resid_ref[...], weight_ref[...], (((1,), (1,)), ((), ())), preferred_element_type=f32
+    )
+    norm_grad = mix_grad * norm_sig * (1.0 + norm_pre * (1.0 - norm_sig)) * gain_ref[...]
+    stat_ref[0] = two_rows(
+        jnp.sum(norm_grad, axis=1, keepdims=True),
+        jnp.sum(norm_grad * normed, axis=1, keepdims=True),
+    )
+    stat_copies = share_sums(stat_ref, stat_send, stat_recv, me_s, me_t, tp)
+    means = summed(stat_ref, stat_copies).T / channels
+    ext_ref[0:tok_rows, :] = row_rstd * (norm_grad - means[:, 0:1] - normed * means[:, 1:2])
+    halo = remote(
+        ext_ref.at[0:halo_rows, :],
+        halo_ref,
+        halo_send,
+        halo_recv,
+        (lax.rem(me_s + sp - 1, sp), me_t),
+    )
+    halo.start()
+
+    chunk = 64 if tok_rows % 64 == 0 else tok_rows
+    starts = list(range(0, tok_rows, chunk))
+
+    def convolve(start):
+        glu_grad = jnp.zeros((chunk, own_channels), f32)
+        for lag_index in range(taps_count):
+            begin = start + taps_count - 1 - lag_index
+            glu_grad = glu_grad + taps_ref[lag_index, :][None, :] * ext_ref[
+                begin : begin + chunk, :
+            ]
+        at = slice(start, start + chunk)
+        gate_sig = jax.nn.sigmoid(gate_ref[at, :].astype(f32))
+        value_out[at, :] = (glu_grad * gate_sig).astype(bf16)
+        gate_out[at, :] = (
+            glu_grad * value_ref[at, :].astype(f32) * gate_sig * (1.0 - gate_sig)
+        ).astype(bf16)
+
+    early = [start for start in starts if start + chunk + taps_count - 1 <= tok_rows]
+    for i in range(max(len(order), len(early))):
+        if i < len(order) and pairs == 2:
+            pass_on(order[i])
+        if i < len(early):
+            convolve(early[i])
+    halo.wait_recv()
+    ext_ref[tok_rows : tok_rows + halo_rows, :] = jnp.where(me_s == sp - 1, 0.0, halo_ref[...])
+    for start in starts[len(early) :]:
+        convolve(start)
+
+    total = proj_ref[me_s]
+    if pairs == 2:
+        total = total + near_ref[0].astype(f32)
+    for d in order[:-1]:
+        far[d].wait_recv()
+        total = total + far_ref[d // 2].astype(f32)
+    weight_out[...] = total
+    for copy in [halo, *stat_copies, *near.values(), *far.values()]:
+        copy.wait_send()
+
+
+def run_conv(resid, stats, conv, value, gate, taps, gain, bias, weight, sp, tp):
+    tok_rows, own_channels = conv.shape
+    share = resid.shape[1] // sp
+    vmem = pl.BlockSpec(memory_space=pltpu.VMEM)
+    dma = pltpu.SemaphoreType.DMA
+    half = max(1, sp // 2)
+    halo_rows = -(-(taps.shape[0] - 1) // 8) * 8
+    return pl.pallas_call(
+        functools.partial(conv_kernel, sp, tp),
+        out_shape=(
+            jax.ShapeDtypeStruct((share, own_channels), f32),
+            jax.ShapeDtypeStruct(conv.shape, bf16),
+            jax.ShapeDtypeStruct(conv.shape, bf16),
+        ),
+        in_specs=[vmem] * 9,
+        out_specs=(vmem,) * 3,
+        scratch_shapes=[
+            pltpu.VMEM((sp, share, own_channels), f32),
+            pltpu.VMEM((sp, share, own_channels), bf16),
+            pltpu.VMEM((half, share, own_channels), bf16),
+            pltpu.VMEM((half, share, own_channels), bf16),
+            pltpu.VMEM((half, share, own_channels), bf16),
+            pltpu.VMEM((tok_rows + halo_rows, own_channels), f32),
+            pltpu.VMEM((halo_rows, own_channels), f32),
+            pltpu.VMEM((tp, 8, tok_rows), f32),
+            dma((half,)),
+            dma((half,)),
+            dma((half,)),
+            dma((half,)),
+            dma(()),
+            dma(()),
+            dma((tp,)),
+            dma((tp,)),
+        ],
+        compiler_params=pltpu.CompilerParams(
+            collective_id=1, has_side_effects=True, vmem_limit_bytes=40 * 1024 * 1024
+        ),
+    )(resid, stats, conv, value, gate, taps, gain, bias, weight)
 
 
 def on_device(
@@ -356,7 +547,7 @@
         )
         for k in range(top_count)
     ).astype(jnp.bfloat16)
-    resid_grad, gate_grad, up_grad, down_grad = run_experts(
+    resid_grad, gate_grad, up_grad, down_grad, row_stats = run_experts(
         send_rows,
         send_cot,
         expert_gate,
@@ -364,51 +555,23 @@
         expert_down,
         picks,
         own_cot,
+        conv_out,
         sp_count,
         tp_count,
     )
-    mix_grad = lax.dot_general(
-        resid_grad, out_weight, (((1,), (1,)), ((), ())), preferred_element_type=jnp.float32
-    )
-    channels = conv_out.shape[1] * tp_count
-    conv_vals = conv_out.astype(jnp.float32)
-    row_sum, row_square = lax.psum(
-        (jnp.sum(conv_vals, axis=1), jnp.sum(conv_vals * conv_vals, axis=1)), "tp"
-    )
-    row_mean = (row_sum / channels)[:, None]
-    row_var = (row_square / channels)[:, None] - row_mean * row_mean
-    row_rstd = lax.rsqrt(row_var + norm_eps)
-    normed = (conv_vals - row_mean) * row_rstd
-    norm_pre = normed * norm_gain[None, :] + norm_bias[None, :]
-    norm_sig = jax.nn.sigmoid(norm_pre)
-    conv_act = (norm_pre * norm_sig).astype(jnp.bfloat16)
-    norm_grad = mix_grad * norm_sig * (1.0 + norm_pre * (1.0 - norm_sig)) * norm_gain[None, :]
-    grad_sum, grad_dot = lax.psum(
-        (jnp.sum(norm_grad, axis=1), jnp.sum(norm_grad * normed, axis=1)), "tp"
-    )
-    conv_grad = row_rstd * (
-        norm_grad - (grad_sum / channels)[:, None] - normed * (grad_dot / channels)[:, None]
-    )
-    taps_count = conv_taps.shape[0]
-    next_rows = passed_along(conv_grad[: taps_count - 1], "sp", -1)
-    extended = jnp.concatenate([conv_grad, next_rows], axis=0)
-    glu_grad = jnp.zeros_like(conv_grad)
-    for lag_index in range(taps_count):
-        begin = taps_count - 1 - lag_index
-        glu_grad = glu_grad + conv_taps[lag_index][None, :] * extended[begin : begin + tok_rows]
-    gate_sig_in = jax.nn.sigmoid(conv_gate.astype(jnp.float32))
-    value_grad = (glu_grad * gate_sig_in).astype(jnp.bfloat16)
-    gate_in_grad = (
-        glu_grad * conv_value.astype(jnp.float32) * gate_sig_in * (1.0 - gate_sig_in)
-    ).astype(jnp.bfloat16)
-    projected = lax.psum_scatter(
-        lax.dot_general(
-            resid_grad, conv_act, (((0,), (0,)), ((), ())), preferred_element_type=jnp.float32
-        ).astype(jnp.bfloat16),
-        "sp",
-        scatter_dimension=0,
-        tiled=True,
-    ).astype(jnp.float32)
+    projected, value_grad, gate_in_grad = run_conv(
+        resid_grad,
+        row_stats,
+        conv_out,
+        conv_value,
+        conv_gate,
+        conv_taps,
+        norm_gain[None, :],
+        norm_bias[None, :],
+        out_weight,
+        sp_count,
+        tp_count,
+    )
     out_weight_grad = projected.T
     return (gate_grad, up_grad, down_grad, resid_grad, out_weight_grad, value_grad, gate_in_grad)
 

time: 230 us -> 171 us (0.74)
  waiting for transfers between devices: 45 us -> 0 us
  Pallas kernels: 119 us -> 144 us
  blocking collectives: 15.1 us -> 0 us
  between operations: 14.2 us -> 0.78 us
  other arithmetic: 11.5 us -> 4.05 us
  matrix products: 10.8 us -> 4.74 us
  local copies, waits for them, and re-layouts: 12.7 us -> 17.2 us
    reduce_scatter x1 -> x0, waiting for transfers between devices: 42.5 us -> none  [on_device(): lax.psum_scatter(lax.dot_general(resid_grad, conv_act, (((0,), (0,)), (()...]
    pallas_call x0 -> x1, Pallas kernels: none -> 23 us  [run_conv(): pl.pallas_call(functools.partial(conv_kernel, sp, tp), out_shape=(jax.Sha...]
    psum x2 -> x0, blocking collectives: 15.1 us -> none  [the longest x1 8.33 us: on_device(): lax.psum((jnp.sum(conv_vals, axis=1), jnp.sum(conv_vals * conv_vals, axis...]
    unnamed x23 -> x35, local copies, waits for them, and re-layouts: 8.88 us -> 15.3 us
    dot_general x2 -> x0, matrix products: 6.09 us -> none  [the longest x1 3.41 us: on_device(): lax.dot_general(resid_grad, conv_act, (((0,), (0,)), ((), ())), preferred...]
    convert_element_type x2 -> x0, other arithmetic: 4.35 us -> none  [the longest x1 3.56 us: on_device(): gate_in_grad = (glu_grad * conv_value.astype(jnp.float32) * gate_sig_in *...]
    ppermute x1 -> x0, waiting for transfers between devices: 2.5 us -> none  [passed_along(): lax.ppermute(value, axis, [(source, source + steps) for source in range(l...]
  transfers between devices with their start and end apart: 2 -> 0, of which waited for: 2 -> 0; matrix products, arithmetic and copies ran while one was open for 5% -> 0% of each run, Pallas kernels for 0% -> 0%
where the time goes in v3:
time: 171 us; the launch traced here: 170 us
  Pallas kernels  144 us (84%)
  local copies, waits for them, and re-layouts  17.2 us (10%)
  matrix products  4.74 us (3%)
  other arithmetic  4.05 us (2%)
    pallas_call x1, Pallas kernels, run_experts(): pl.pallas_call(functools.partial(expert_kernel, sp, tp), out_shape=(jax.S...  121 us
    pallas_call x1, Pallas kernels, run_conv(): pl.pallas_call(functools.partial(conv_kernel, sp, tp), out_shape=(jax.Sha...  23 us
    unnamed x35, local copies, waits for them, and re-layouts  15.3 us
    dot_general x3, matrix products, chosen(): jnp.einsum('setr,td->serd', which, values, preferred_element_type=jnp.flo...  4.6 us

profile of v3, /device:TPU:0, one launch (start us, length us, event | category | flops | bytes accessed | tf_op | source)
XLA Modules:
  0.0 170.3 jit_solution(13384439705195022738)
XLA Ops:
  0.6 0.0 copy-start
  0.7 0.8 fusion.40
  1.5 0.8 slice_reduce_fusion.2
  2.2 0.1 fusion.31
  2.4 0.8 select_reduce_fusion
  3.1 0.7 convert_add_fusion
  3.9 1.0 constant_dynamic-slice_fusion.refs_6_
  4.9 0.0 copy-done
  4.9 0.0 copy-start.11
  4.9 1.9 %fusion.15.refs_0_ = bf16[8,1,144,512]{3,2,1,0:T(8,128)(2,1)} fusion(s32[384]{0:T(512)S(1)} %get-tuple-element.40, s32[8]{0:T(128)S(1)} %iota_multiply_fusion, s32[384]{0:T(512)S(1)} %get-tuple-element.39, bf16[384,2048]{1,0:T(8,128)(2,1)S(1)} %copy-done, s32[]{:T(128)S(6)} %select_n.9), kind=kOutput, calls=%fused_computation.15 | convolution fusion | flops 457555968 | bytes 1577476 | tf_op jit(solution)/shard_map/setr,td->serd/dot_general | solution.py:540
  6.8 1.8 %fusion.12.refs_5_ = bf16[8,1,384,144]{3,2,1,0:T(8,128)(2,1)} fusion(s32[384]{0:T(512)S(1)} %get-tuple-element.40, s32[8]{0:T(128)S(1)} %iota_multiply_fusion, s32[384]{0:T(512)S(1)} %get-tuple-element.39), kind=kLoop, calls=%fused_computation.13 | loop fusion | flops 3981312 | bytes 887840 | tf_op jit(solution)/shard_map/add | solution.py:534
  8.6 0.9 fusion.6
  9.4 0.0 copy-done.11
  9.4 1.9 %fusion.16.refs_1_ = bf16[8,1,144,512]{3,2,1,0:T(8,128)(2,1)} fusion(f32[8,144,512]{2,1,0:T(8,128)S(1)} %fusion.6, s32[384]{0:T(512)S(1)} %get-tuple-element.40, s32[8]{0:T(128)S(1)} %iota_multiply_fusion, bf16[384,512]{1,0:T(8,128)(2,1)S(1)} %constant_dynamic-slice_fusion.refs_6_, f32[384]{0:T(512)S(1)} %get-tuple-element.37), kind=kOutput, calls=%fused_computation.16 | convolution fusion | flops 455639040 | bytes 3935264 | tf_op jit(solution)/shard_map/setr,td->serd/dot_general | solution.py:540
  11.3 0.0 copy-start.4
  11.3 0.0 copy-start.5
  11.3 0.0 copy-start.7
  11.3 0.0 copy-start.9
  11.3 0.0 copy-start.10
  11.3 120.5 %shard_map.189 = (bf16[384,2048]{1,0:T(8,128)(2,1)}, f32[1,2048,256]{2,1,0:T(8,128)}, f32[1,2048,256]{2,1,0:T(8,128)}, f32[1,256,2048]{2,1,0:T(8,128)}, f32[8,384]{1,0:T(8,128)}) custom-call(bf16[8,1,144,512]{3,2,1,0:T(8,128)(2,1)} %fusion.15.refs_0_, bf16[8,1,144,512]{3,2,1,0:T(8,128)(2,1)} %fusion.16.refs_1_, bf16[1,2048,256]{2,1,0:T(8,128)(2,1)} %refs_2_.2, ...), custom_call_target="tpu_custom_call" | custom-call | tf_op jit(solution)/shard_map/pallas_call | solution.py:299
  131.9 0.0 copy-done.4
  131.9 0.0 copy-done.5
  131.9 0.0 copy-done.7
  131.9 0.0 copy-done.9
  131.9 0.0 copy-done.10
  131.9 0.0 copy-start.1
  131.9 1.4 copy-done.1
  133.3 0.0 copy-start.3
  133.3 1.2 copy-done.3
  134.6 0.0 copy-start.6
  134.6 0.9 copy-done.6
  135.5 0.0 copy-start.8
  135.5 0.7 copy-done.8
  136.2 23.0 %shard_map.190 = (f32[256,256]{1,0:T(8,128)S(1)}, bf16[384,256]{1,0:T(8,128)(2,1)S(1)}, bf16[384,256]{1,0:T(8,128)(2,1)S(1)}) custom-call(bf16[384,2048]{1,0:T(8,128)(2,1)S(1)} %copy-done.1, f32[8,384]{1,0:T(8,128)S(1)} %copy-done.8, bf16[384,256]{1,0:T(8,128)(2,1)S(1)} %copy-done.4, bf16[384,256]{1,0:T(8,128)(2,1)S(1)} %copy-done.5, ...), custom_call_target="tpu_custom_call" | custom-call | tf_op jit(solution)/shard_map/pallas_call | solution.py:461
  159.2 0.8 copy.24
  160.1 0.0 copy-start.13
  160.1 3.2 %copy.31 = f32[1,2048,256]{2,1,0:T(8,128)} copy(f32[1,2048,256]{2,1,0:T(8,128)} %get-tuple-element.48) | data formatting | bytes 4194304
  163.3 0.0 copy-done.13
  163.3 0.0 copy-start.12
  163.3 1.3 copy.32
  164.6 1.0 copy-done.12
  165.6 0.0 copy-start.2
  165.6 1.3 copy.33
  166.9 0.8 copy-done.2
  167.8 1.1 copy.34
  168.9 0.7 copy.35
  169.6 0.7 copy.36
  (2 shorter events, 0.0 us)
Async XLA Ops:
  0.6 4.3 %copy-start = (bf16[384,2048]{1,0:T(8,128)(2,1)S(1)}, bf16[384,2048]{1,0:T(8,128)(2,1)}, u32[]{:S(2)}) copy-start(bf16[384,2048]{1,0:T(8,128)(2,1)} %param.14) | copy-start | bytes 4718596
  4.9 4.5 %copy-start.11 = (bf16[384,512]{1,0:T(8,128)(2,1)}, bf16[384,512]{1,0:T(8,128)(2,1)S(1)}, u32[]{:S(2)}) copy-start(bf16[384,512]{1,0:T(8,128)(2,1)S(1)} %constant_dynamic-slice_fusion.refs_6_) | copy-start | bytes 1179652
  11.3 120.6 %copy-start.4 = (bf16[384,256]{1,0:T(8,128)(2,1)S(1)}, bf16[384,256]{1,0:T(8,128)(2,1)}, u32[]{:S(2)}) copy-start(bf16[384,256]{1,0:T(8,128)(2,1)} %refs_2_.3) | copy-start | bytes 589828
  11.3 120.6 %copy-start.5 = (bf16[384,256]{1,0:T(8,128)(2,1)S(1)}, bf16[384,256]{1,0:T(8,128)(2,1)}, u32[]{:S(2)}) copy-start(bf16[384,256]{1,0:T(8,128)(2,1)} %refs_3_.3) | copy-start | bytes 589828
  11.3 120.6 %copy-start.7 = (f32[31,256]{1,0:T(8,128)S(1)}, f32[31,256]{1,0:T(8,128)}, u32[]{:S(2)}) copy-start(f32[31,256]{1,0:T(8,128)} %refs_5_.1) | copy-start | bytes 95236
  11.3 120.6 %copy-start.9 = (f32[256]{0:T(256)S(1)}, f32[256]{0:T(256)}, u32[]{:S(2)}) copy-start(f32[256]{0:T(256)} %param.25) | copy-start | bytes 3076
  11.3 120.6 %copy-start.10 = (f32[256]{0:T(256)S(1)}, f32[256]{0:T(256)}, u32[]{:S(2)}) copy-start(f32[256]{0:T(256)} %param.26) | copy-start | bytes 3076
  131.9 1.4 copy-start.1
  133.3 1.2 copy-start.3
  134.6 0.9 copy-start.6
  135.5 0.7 copy-start.8
  160.1 3.2 %copy-start.13 = (f32[1,2048,256]{2,1,0:T(8,128)S(1)}, f32[1,2048,256]{2,1,0:T(8,128)}, u32[]{:S(2)}) copy-start(f32[1,2048,256]{2,1,0:T(8,128)} %get-tuple-element.49) | copy-start | bytes 6291460
  163.3 2.3 %copy-start.12 = (f32[1,256,2048]{2,1,0:T(8,128)S(1)}, f32[1,256,2048]{2,1,0:T(8,128)}, u32[]{:S(2)}) copy-start(f32[1,256,2048]{2,1,0:T(8,128)} %get-tuple-element.50) | copy-start | bytes 6291460
  165.6 2.2 %copy-start.2 = (bf16[384,2048]{1,0:T(8,128)(2,1)S(1)}, bf16[384,2048]{1,0:T(8,128)(2,1)}, u32[]{:S(2)}) copy-start(bf16[384,2048]{1,0:T(8,128)(2,1)} %get-tuple-element.51.refs_0_) | copy-start | bytes 4718596
